TPU v7x, 128 devices: a whole 4x4x4 slice. The times are simulated.
128 devices in a mesh: st: 16 (over z, x), tp: 8 (over y, core).
Axes of the slice: x: 4, y: 4, z: 4, core: 2. Of those that a mesh axis runs over, the one named last changes fastest.
Arguments:
- tokens: bfloat16 [32768, 2048], P('st', 'tp'), may hold values from -48 to 48
- store: bfloat16 [512, 64, 2048], P('st'), may hold values from -48 to 48
- passage_holder_index: int32 [256, 2], P('st'), may hold values from 0 to 15, all different within a row; in each aligned block of 16 rows (0 to 15, 16 to 31, ...) at most 4 rows name the same one
- passage_slot: int32 [256, 2], P('st'), may hold values from 0 to 31
- query_weight: bfloat16 [2048, 1024], P(None, 'tp'), may hold values from -0.125 to 0.125
- key_matrix: bfloat16 [2048, 1024], P(None, 'tp'), may hold values from -0.125 to 0.125
- value_weight: bfloat16 [2048, 1024], P(None, 'tp'), may hold values from -0.125 to 0.125
- outer_gate: bfloat16 [2048, 1024], P(None, 'tp'), may hold values from -0.125 to 0.125
- inner_gate: bfloat16 [2048, 1024], P(None, 'tp'), may hold values from -0.125 to 0.125
- conv_input: bfloat16 [2048, 1024], P(None, 'tp'), may hold values from -0.125 to 0.125
- conv_taps: bfloat16 [3, 1024], P(None, 'tp'), may hold values from -3.5 to 3.5
- route_gate_projection: bfloat16 [2048, 2], replicated, may hold values from -0.125 to 0.125
- conv_out: bfloat16 [1024, 2048], P('tp'), may hold values from -0.1875 to 0.1875
- memory_out: bfloat16 [1024, 2048], P('tp'), may hold values from -0.1875 to 0.1875
Outputs:
- mixed: bfloat16 [32768, 2048], P(('st', 'tp'))
Inputs may be any that keep to these rules, and one draw needn't show every extreme that they name: `passage_holder_index`: each row names 2 different owners; among the rows of one index of st (16 aligned rows) no owner is named more than 4 times, a bound that some index of st reaches.
All inputs are finite; a program needn't handle non-finite values.
Results may differ from a plain program's by a relative error of at most 0.014.
Values may be sent and summed in bfloat16 or wider, within the bound.
A program may use at most 128 MiB of HBM per device.

v0:
```python
import jax
import jax.numpy as jnp
from jax import lax
from jax.sharding import PartitionSpec as P

HEAD_SIZE = 128
CONV_K = 3
SEQ_LEN = 256
BLOCK = 128
NPB = 2
PLEN = 64


def local(
    tokens,
    store,
    passage_holder_index,
    passage_slot,
    query_weight,
    key_matrix,
    value_weight,
    outer_gate,
    inner_gate,
    conv_input,
    conv_taps,
    route_gate_projection,
    conv_out,
    memory_out,
):
    row_count = tokens.shape[0]
    head_width = query_weight.shape[1]
    local_heads = head_width // HEAD_SIZE
    conv_cols = outer_gate.shape[1]
    local_weight = jnp.concatenate([query_weight, outer_gate, inner_gate, conv_input], axis=1)
    pieces = lax.all_gather(tokens, "tp", axis=1, tiled=True)
    projected = jnp.dot(pieces, local_weight, preferred_element_type=jnp.float32)
    gate_logits = jnp.dot(pieces, route_gate_projection, preferred_element_type=jnp.float32)
    queries = projected[:, :head_width].astype(jnp.bfloat16)
    outer_part = projected[:, head_width : head_width + conv_cols]
    inner_part = projected[:, head_width + conv_cols : head_width + 2 * conv_cols]
    value_part = projected[:, head_width + 2 * conv_cols :]
    branch_mix = jax.nn.sigmoid(gate_logits)
    seq_count = row_count // SEQ_LEN
    mixed_input = (inner_part * value_part).reshape(seq_count, SEQ_LEN, conv_cols)
    padded_input = jnp.pad(mixed_input, ((0, 0), (CONV_K - 1, 0), (0, 0)))
    tap_values = conv_taps.astype(jnp.float32)
    filtered_signal = tap_values[0] * padded_input[:, 0:SEQ_LEN]
    for offset in range(1, CONV_K):
        filtered_signal = (
            filtered_signal + tap_values[offset] * padded_input[:, offset : offset + SEQ_LEN]
        )
    conv_branch = (outer_part * filtered_signal.reshape(row_count, conv_cols)).astype(jnp.bfloat16)
    owners = passage_holder_index.reshape(-1)
    local_slots = passage_slot.reshape(-1)
    block_count = passage_holder_index.shape[0]
    owner_count = lax.axis_size("st")
    request_count = owners.shape[0]
    capacity = max(2, 2 * request_count // owner_count)
    one_hot = (owners[:, None] == jnp.arange(owner_count, dtype=jnp.int32)[None, :]).astype(
        jnp.int32
    )
    before = jnp.cumsum(one_hot, axis=0) - one_hot
    position = jnp.sum(before * one_hot, axis=1)
    target = owners * capacity + position
    matches = (
        target[:, None] == jnp.arange(owner_count * capacity, dtype=jnp.int32)[None, :]
    ).astype(jnp.int32)
    outgoing = jnp.sum(matches * local_slots[:, None], axis=0).reshape(owner_count, capacity)
    wanted = lax.all_to_all(outgoing, "st", split_axis=0, concat_axis=0, tiled=True)
    flat_rows = store.reshape(-1, store.shape[-1])
    key_part = jnp.dot(flat_rows, key_matrix, preferred_element_type=jnp.float32).astype(
        jnp.bfloat16
    )
    retrieved_content_vectors = jnp.dot(
        flat_rows, value_weight, preferred_element_type=jnp.float32
    ).astype(jnp.bfloat16)
    joined = jnp.concatenate([key_part, retrieved_content_vectors], axis=1)
    table = joined.reshape(store.shape[:-1] + (2 * head_width,))
    chosen = table[wanted.reshape(-1)].reshape(wanted.shape + table.shape[1:])
    served = lax.all_to_all(chosen, "st", split_axis=0, concat_axis=0, tiled=True)
    slot_table = served.reshape(owner_count * capacity, PLEN, 2 * head_width)
    picked = slot_table[target].reshape(block_count, NPB * PLEN, 2 * head_width)
    passage_key_rows = picked[:, :, :head_width].reshape(
        block_count, NPB * PLEN, local_heads, HEAD_SIZE
    )
    retrieved_content_vectors = picked[:, :, head_width:].reshape(
        block_count, NPB * PLEN, local_heads, HEAD_SIZE
    )
    query_block_rows = queries.reshape(block_count, BLOCK, local_heads, HEAD_SIZE)
    scores = jnp.einsum(
        "xuhd,xkhd->xhuk", query_block_rows, passage_key_rows, preferred_element_type=jnp.float32
    ) * HEAD_SIZE ** (-0.5)
    softmax_shares = jax.nn.softmax(scores, axis=-1).astype(jnp.bfloat16)
    memory_branch = jnp.einsum(
        "xhuk,xkhd->xuhd",
        softmax_shares,
        retrieved_content_vectors,
        preferred_element_type=jnp.float32,
    )
    memory_branch = memory_branch.reshape(row_count, head_width).astype(jnp.bfloat16)
    return lax.psum_scatter(
        (
            branch_mix[:, 0:1] * jnp.dot(conv_branch, conv_out, preferred_element_type=jnp.float32)
            + branch_mix[:, 1:2]
            * jnp.dot(memory_branch, memory_out, preferred_element_type=jnp.float32)
        ).astype(jnp.bfloat16),
        "tp",
        scatter_dimension=0,
        tiled=True,
    )


def solution(mesh):
    return jax.shard_map(
        local,
        mesh=mesh,
        in_specs=(
            P("st", "tp"),
            P("st", None, None),
            P("st", None),
            P("st", None),
            P(None, "tp"),
            P(None, "tp"),
            P(None, "tp"),
            P(None, "tp"),
            P(None, "tp"),
            P(None, "tp"),
            P(None, "tp"),
            P(),
            P("tp", None),
            P("tp", None),
        ),
        out_specs=P(("st", "tp"), None),
        check_vma=False,
    )
```

profile of v0, /device:TPU:1, one launch (start us, length us, event | category | flops | bytes accessed | tf_op | source)
XLA Modules:
  0.0 160.1 jit_solution(17596449766068690858)
XLA Ops:
  6.5 0.7 all-gather.2.cloned.1.call-update
  7.3 0.8 copy.35
  8.0 0.1 mul.118
  8.1 0.8 copy.34
  8.9 0.1 reshape.135
  9.0 0.1 fusion.23
  9.0 0.1 reduce_window_sum.11
  9.1 0.2 select_reduce_fusion.1
  9.3 0.1 select_reduce_fusion
  9.4 0.7 all_to_all.9
  10.1 8.4 %all-to-all-start = ((s32[16,1,4]{2,1,0:T(1,128)}), s32[16,1,4]{2,1,0:T(1,128)S(1)}, u32[]{:S(2)}, u32[]{:S(2)}) async-start(s32[16,1,4]{2,1,0:T(1,128)} %bitcast.8), calls=%async_computation | async-start | bytes 16384 | tf_op jit(solution)/shard_map/all_to_all | solution.py:69
  18.5 0.0 copy-start.1
  18.5 0.0 copy-start.5
  18.5 6.8 %convolution_convert_fusion = bf16[2048,128]{0,1:T(8,128)(2,1)S(1)} fusion(bf16[2048,2048]{1,0:T(8,128)(2,1)} %bitcast.51, bf16[2048,128]{1,0:T(8,128)(2,1)} %param.20), kind=kOutput, calls=%fused_computation.5 | convolution fusion | flops 1074003968 | bytes 9437184 | tf_op jit(solution)/shard_map/dot_general | solution.py:74
  25.4 0.2 copy-done.1
  25.6 0.1 copy-done.5
  25.6 2.9 %convolution_convert_fusion.1 = bf16[2048,128]{0,1:T(8,128)(2,1)S(1)} fusion(bf16[2048,2048]{1,0:T(8,128)(2,1)S(1)} %bitcast.52, bf16[2048,128]{1,0:T(8,128)(2,1)S(1)} %copy-done.5), kind=kOutput, calls=%fused_computation.6 | convolution fusion | flops 1074003968 | bytes 9437184 | tf_op jit(solution)/shard_map/dot_general | solution.py:71
  28.5 0.1 pad_maximum_fusion
  28.7 0.5 copy.33
  29.2 0.5 broadcast.75
  29.7 0.7 reduce.7
  30.4 0.1 reshape.136
  30.5 0.0 copy-start.8
  30.5 0.0 copy-start.7
  30.5 2.1 %gather_fusion = bf16[64,64,256]{2,1,0:T(8,128)(2,1)} fusion(bf16[32,64,256]{2,1,0:T(8,128)(2,1)S(1)} %bitcast.53, s32[1024]{0:T(1024)S(1)} %pad_clamp_fusion.1), kind=kCustom, calls=%fused_computation | custom fusion | bytes 4194560 | tf_op jit(solution)/shard_map/gather | solution.py:79
  32.6 6.8 %all-to-all-start.1 = ((bf16[16,4,64,256]{3,2,1,0:T(8,128)(2,1)}), bf16[16,4,64,256]{3,2,1,0:T(8,128)(2,1)S(1)}, u32[]{:S(2)}, u32[]{:S(2)}) async-start(bf16[16,4,64,256]{3,2,1,0:T(8,128)(2,1)} %bitcast.54), calls=%async_computation.1 | async-start | bytes 4194304 | tf_op jit(solution)/shard_map/all_to_all | solution.py:80
  39.4 0.2 reduce-scatter.2.cloned.1.call-start
  39.6 0.1 copy.37
  39.7 0.1 mul.123
  39.9 28.3 %all-to-all-done.1 = bf16[16,4,64,256]{3,2,1,0:T(8,128)(2,1)S(1)} async-done(((bf16[16,4,64,256]{3,2,1,0:T(8,128)(2,1)}), bf16[16,4,64,256]{3,2,1,0:T(8,128)(2,1)S(1)}, u32[]{:S(2)}, u32[]{:S(2)}) %all-to-all-start.1) | async-done | bytes 2097184 | tf_op jit(solution)/shard_map/all_to_all | solution.py:80
  68.2 1.6 gather_fusion.1
  69.8 7.6 %convolution_bitcast_fusion = f32[2048,512]{0,1:T(8,128)S(1)} fusion(bf16[2048,2048]{1,0:T(8,128)(2,1)} %all-gather.2.cloned.1.call-done, bf16[2048,128]{1,0:T(8,128)(2,1)S(1)} %copy-done.9, bf16[2048,128]{1,0:T(8,128)(2,1)} %param.22, bf16[2048,128]{1,0:T(8,128)(2,1)} %param.21, bf16[2048,128]{1,0:T(8,128)(2,1)} %param.18), kind=kOutput, calls=%fused_computation.4 | convolution fusion | flops 4303355904 | bytes 14680064 | tf_op jit(solution)/shard_map/dot_general | solution.py:36
  77.4 2.0 %copy-done.2 = f32[2048,512]{0,1:T(8,128)} copy-done((f32[2048,512]{0,1:T(8,128)}, f32[2048,512]{0,1:T(8,128)S(1)}, u32[]{:S(2)}) %copy-start.2) | copy-done | bytes 4194328
  79.3 0.1 slice.94
  79.4 0.0 copy-start.6
  79.4 0.3 copy.41
  79.7 0.5 fusion.32
  80.2 1.4 convolution_multiply_fusion
  81.7 1.7 %slice_multiply_fusion = f32[2048,128]{0,1:T(8,128)S(1)} fusion(f32[2048,512]{0,1:T(8,128)} %copy-done.2), kind=kLoop, calls=%fused_computation.29 | loop fusion | flops 262144 | bytes 3145728 | tf_op jit(solution)/shard_map/mul | solution.py:44
  83.4 5.7 %fusion.3 = f32[2048,2]{0,1:T(2,128)S(1)} fusion(bf16[2048,2048]{1,0:T(8,128)(2,1)} %all-gather.2.cloned.1.call-done, bf16[2048,2]{0,1:T(2,128)(2,1)S(1)} %copy-done.6), kind=kOutput, calls=%fused_computation.10 | convolution fusion | flops 16789504 | bytes 8413184 | tf_op jit(solution)/shard_map/dot_general | solution.py:37
  89.1 0.3 copy.42
  89.4 1.0 fusion.15
  90.4 0.3 copy.43
  90.8 2.0 %convolution_convert_fusion.2 = bf16[16,128,128]{1,2,0:T(8,128)(2,1)S(1)} fusion(bf16[16,128,256]{2,1,0:T(8,128)(2,1)S(1)} %bitcast.62, f32[16,128]{1,0:T(8,128)S(1)} %fusion.32, f32[16,128,128]{1,2,0:T(8,128)} %convolution_multiply_fusion), kind=kOutput, calls=%fused_computation.23 | convolution fusion | flops 68159616 | bytes 3153920 | tf_op jit(solution)/shard_map/xhuk,xkhd->xuhd/dot_general | solution.py:94
  92.8 3.7 %fusion.18 = f32[2048,2048]{1,0:T(8,128)S(1)} fusion(bf16[128,2048]{1,0:T(8,128)(2,1)S(1)} %copy-done, f32[2048,128]{0,1:T(8,128)S(1)} %bitcast.55, f32[2048,512]{0,1:T(8,128)} %copy-done.2), kind=kOutput, calls=%fused_computation.34 | convolution fusion | flops 1074266112 | bytes 19398656 | tf_op jit(solution)/shard_map/dot_general | solution.py:103
  96.5 4.7 %add_convert_fusion = bf16[2048,2048]{1,0:T(8,128)(2,1)} fusion(f32[2048,2048]{1,0:T(8,128)S(1)} %fusion.18, bf16[2048,128]{1,0:T(8,128)(2,1)S(1)} %bitcast.65, bf16[128,2048]{1,0:T(8,128)(2,1)S(1)} %copy-done.4, f32[2048]{0:T(1024)S(1)} %bitcast.67, f32[2048]{0:T(1024)S(1)} %bitcast.66), kind=kOutput, calls=%fused_computation.3 | convolution fusion | flops 1090519040 | bytes 26230784 | tf_op jit(solution)/shard_map/dot_general | solution.py:105
  101.1 0.0 reduce-scatter.2.cloned.1.call-update
  101.2 52.1 %reduce-scatter.2.cloned.1.call-done = bf16[256,2048]{1,0:T(8,128)(2,1)} async-done(((bf16[2048,2048]{1,0:T(8,128)(2,1)}), bf16[256,2048]{1,0:T(8,128)(2,1)}) %reduce-scatter.2.cloned.1.call-update) | async-done | bytes 1048592 | tf_op jit(solution)/shard_map/reduce_scatter | solution.py:101
  (24 shorter events, 0.1 us)
Async XLA Ops:
  6.5 86.3 %copy-start = (bf16[128,2048]{1,0:T(8,128)(2,1)S(1)}, bf16[128,2048]{1,0:T(8,128)(2,1)}, u32[]{:S(2)}) copy-start(bf16[128,2048]{1,0:T(8,128)(2,1)} %param.26) | copy-start | bytes 1572868
  6.5 63.2 %all-gather.2.cloned.1.call-start = ((), (), s32[]{:S(2)}) async-start(), calls=%async_computation.3 | async-start | bytes 9437184 | tf_op jit(solution)/shard_map/all_gather | solution.py:35
  10.1 19.1 %all-to-all-start = ((s32[16,1,4]{2,1,0:T(1,128)}), s32[16,1,4]{2,1,0:T(1,128)S(1)}, u32[]{:S(2)}, u32[]{:S(2)}) async-start(s32[16,1,4]{2,1,0:T(1,128)} %bitcast.8), calls=%async_computation | async-start | bytes 16384 | tf_op jit(solution)/shard_map/all_to_all | solution.py:69
  18.5 7.1 %copy-start.1 = (bf16[32,64,2048]{2,1,0:T(8,128)(2,1)S(1)}, bf16[32,64,2048]{2,1,0:T(8,128)(2,1)}, u32[]{:S(2)}) copy-start(bf16[32,64,2048]{2,1,0:T(8,128)(2,1)} %param.15) | copy-start | bytes 25165828
  18.5 7.1 %copy-start.5 = (bf16[2048,128]{1,0:T(8,128)(2,1)S(1)}, bf16[2048,128]{1,0:T(8,128)(2,1)}, u32[]{:S(2)}) copy-start(bf16[2048,128]{1,0:T(8,128)(2,1)} %param.19) | copy-start | bytes 1572868
  30.5 9.1 %copy-start.8 = (bf16[3,128]{1,0:T(4,128)(2,1)S(1)}, bf16[3,128]{1,0:T(4,128)(2,1)}, u32[]{:S(2)}) copy-start(bf16[3,128]{1,0:T(4,128)(2,1)} %param.24) | copy-start | bytes 2308
  30.5 9.1 %copy-start.7 = (s32[16,2]{0,1:T(2,128)S(1)}, s32[16,2]{0,1:T(2,128)}, u32[]{:S(2)}) copy-start(s32[16,2]{0,1:T(2,128)} %param.16) | copy-start | bytes 388
  32.6 37.2 %copy-start.9 = (bf16[2048,128]{1,0:T(8,128)(2,1)S(1)}, bf16[2048,128]{1,0:T(8,128)(2,1)}, u32[]{:S(2)}) copy-start(bf16[2048,128]{1,0:T(8,128)(2,1)} %param.23) | copy-start | bytes 1572868
  32.6 35.6 %all-to-all-start.1 = ((bf16[16,4,64,256]{3,2,1,0:T(8,128)(2,1)}), bf16[16,4,64,256]{3,2,1,0:T(8,128)(2,1)S(1)}, u32[]{:S(2)}, u32[]{:S(2)}) async-start(bf16[16,4,64,256]{3,2,1,0:T(8,128)(2,1)} %bitcast.54), calls=%async_computation.1 | async-start | bytes 4194304 | tf_op jit(solution)/shard_map/all_to_all | solution.py:80
  39.4 113.9 %reduce-scatter.2.cloned.1.call-start = ((), (), s32[]{:S(2)}) async-start(), calls=%async_computation.4 | async-start | bytes 9437184 | tf_op jit(solution)/shard_map/reduce_scatter | solution.py:101
  69.8 9.9 %copy-start.3 = (bf16[32,64,256]{2,1,0:T(8,128)(2,1)S(1)}, bf16[32,64,256]{2,1,0:T(8,128)(2,1)}, u32[]{:S(2)}) copy-start(bf16[32,64,256]{2,1,0:T(8,128)(2,1)} %gather_fusion.1) | copy-start | bytes 3145732
  77.4 2.0 %copy-start.2 = (f32[2048,512]{0,1:T(8,128)}, f32[2048,512]{0,1:T(8,128)S(1)}, u32[]{:S(2)}) copy-start(f32[2048,512]{0,1:T(8,128)S(1)} %convolution_bitcast_fusion) | copy-start | bytes 12582916
  79.4 4.0 %copy-start.6 = (bf16[2048,2]{0,1:T(2,128)(2,1)S(1)}, bf16[2048,2]{0,1:T(2,128)(2,1)}, u32[]{:S(2)}) copy-start(bf16[2048,2]{0,1:T(2,128)(2,1)} %param.25) | copy-start | bytes 24580
  92.8 3.7 %copy-start.4 = (bf16[128,2048]{1,0:T(8,128)(2,1)S(1)}, bf16[128,2048]{1,0:T(8,128)(2,1)}, u32[]{:S(2)}) copy-start(bf16[128,2048]{1,0:T(8,128)(2,1)} %param.27) | copy-start | bytes 1572868
Sparse Core Ops, SparseCore 0:
  9.0 57.0 all-gather.1
  101.3 51.9 reduce-scatter.1
where the time goes:
time: 160 us
  waiting for transfers between devices  81.2 us (51%)
  matrix products  35.3 us (22%)
  starting transfers between devices  15.4 us (10%)
  between operations  13.7 us (9%)
  local copies, waits for them, and re-layouts  10.7 us (7%)
  other arithmetic  3.89 us (2%)
    reduce_scatter x1, waiting for transfers between devices, local(): lax.psum_scatter((branch_mix[:, 0:1] * jnp.dot(conv_branch, conv_out, pre...  52.1 us
    all_to_all x1, waiting for transfers between devices, local(): lax.all_to_all(chosen, 'st', split_axis=0, concat_axis=0, tiled=True)  28.3 us
    all_to_all x1, starting transfers between devices, local(): lax.all_to_all(outgoing, 'st', split_axis=0, concat_axis=0, tiled=True)  8.42 us
    dot_general x1, matrix products, local(): jnp.dot(pieces, local_weight, preferred_element_type=jnp.float32)  7.57 us
    dot_general x1, matrix products, local(): jnp.dot(flat_rows, value_weight, preferred_element_type=jnp.float32)  6.83 us
    all_to_all x1, starting transfers between devices, local(): lax.all_to_all(chosen, 'st', split_axis=0, concat_axis=0, tiled=True)  6.77 us
    dot_general x1, matrix products, local(): jnp.dot(pieces, route_gate_projection, preferred_element_type=jnp.float32)  5.66 us
    dot_general x1, matrix products, local(): jnp.dot(memory_branch, memory_out, preferred_element_type=jnp.float32)  4.67 us
  transfers between devices with their start and end apart: 4, of which 2 were waited for; matrix products, arithmetic and copies ran while one was open for 11% of the time, Pallas kernels for 0%

commit v1 on v0

v1 whole, which is shorter than its diff:
```python
import jax
import jax.numpy as jnp
from jax import lax
from jax.experimental import pallas as pl
from jax.experimental.pallas import tpu as pltpu
from jax.sharding import PartitionSpec as P

HEAD_SIZE = 128
SEQ = 256
BLOCK = 128
PLEN = 64
CAP = 4
NY = 4
NXZ = 4
NST = 16
NTP = 8
MESH = pl.DeviceIdType.MESH
F32 = jnp.float32
BF16 = jnp.bfloat16


def kernel(
    tokens, store, holder, slot, wq, wo, wi, wv, wk, wval, taps, route, cout, mout,
    out,
    G, ST, WIN, WKV, TB, KS, KR, OV, WV, WS, PV, PS, Q, AS, A, W,
    lsem, stsem, ixr, ixs, kvr, kvs, agr, sib, gsend, arecv, asend,
    wloc, w1, p1, p2, wsib, wsend,
):
    st = lax.axis_index("st")
    tp = lax.axis_index("tp")
    y = lax.div(tp, 2)
    k = lax.rem(tp, 2)
    z = lax.div(st, NXZ)
    x = lax.rem(st, NXZ)
    a = (1 - k) * x + k * z
    b = (1 - k) * z + k * x

    def stidx(aa, bb):
        return (1 - k) * (bb * NXZ + aa) + k * (aa * NXZ + bb)

    def ring(v, d):
        return lax.rem(v + d + 4, 4)

    def dev_y(d):
        return (st, ring(y, d) * 2 + k)

    sibling = (st, y * 2 + (1 - k))

    def rcopy(src, dst, ssem, rsem, dev):
        return pltpu.make_async_remote_copy(
            src_ref=src, dst_ref=dst, send_sem=ssem, recv_sem=rsem,
            device_id=dev, device_id_type=MESH,
        )

    def arrived(ref, sem):
        pltpu.make_async_copy(ref, ref, sem).wait()

    def seq_of(t):
        return lax.rem(t, 4) * 2 + lax.div(t, 4)

    def rows(s, lo=0, n=SEQ):
        return pl.ds(pl.multiple_of(s * SEQ + lo, 64), n)

    loads = []
    for j, w in enumerate((wq, wo, wi, wv)):
        loads.append(pltpu.make_async_copy(w, WIN.at[:, pl.ds(j * 128, 128)], lsem.at[j]))
    for j, w in enumerate((wk, wval)):
        loads.append(pltpu.make_async_copy(w, WKV.at[:, pl.ds(j * 128, 128)], lsem.at[4 + j]))
    own = pltpu.make_async_copy(tokens, G.at[tp], lsem.at[6])
    for c in loads[4:]:
        c.start()

    def store_copy(i):
        r = pl.ds(pl.multiple_of(i * SEQ, SEQ), SEQ)
        return pltpu.make_async_copy(store.at[r, :], ST.at[r, :], stsem.at[i])

    def start_store(i, _):
        store_copy(i).start()
        return 0

    lax.fori_loop(0, 8, start_store, 0)
    for c in loads[:4]:
        c.start()
    own.start()

    def wl(cs, m):
        src = (cout, mout)[m]
        return pltpu.make_async_copy(
            src.at[:, pl.ds(pl.multiple_of(cs * 128, 128), 128)], W.at[cs, k, y, m], wloc.at[0]
        )

    def start_wl(cs, _):
        wl(cs, 0).start()
        wl(cs, 1).start()
        return 0

    lax.fori_loop(0, NST, start_wl, 0)

    bar = pltpu.get_barrier_semaphore()

    def sig_tp(d, _):
        pl.semaphore_signal(bar, inc=1, device_id=(st, lax.rem(tp + d, NTP)), device_id_type=MESH)
        return 0

    def sig_st(d, _):
        pl.semaphore_signal(bar, inc=1, device_id=(lax.rem(st + d, NST), tp), device_id_type=MESH)
        return 0

    lax.fori_loop(1, NTP, sig_tp, 0)
    lax.fori_loop(1, NST, sig_st, 0)

    rowi = lax.broadcasted_iota(jnp.int32, (NST, 128), 0)
    lanei = lax.broadcasted_iota(jnp.int32, (NST, 128), 1)
    count = jnp.zeros((NST, 128), jnp.int32)
    wanted = jnp.zeros((NST, 128), jnp.int32)
    for r in range(32):
        o = holder[r % 2, r // 2]
        v = slot[r % 2, r // 2]
        hit = rowi == o
        PV[r] = jnp.sum(jnp.where(hit, count, 0), axis=0, keepdims=True) + o * CAP
        wanted = jnp.where(hit & (lanei == count), v, wanted)
        count = count + hit.astype(jnp.int32)
    for o in range(NST):
        OV[o] = wanted[o : o + 1]
    pcopy = pltpu.make_async_copy(PV, PS, lsem.at[7])
    pcopy.start()

    pl.semaphore_wait(bar, NTP - 1 + NST - 1)

    def ix_copy(d):
        r = lax.rem(st + d, NST)
        return rcopy(OV.at[r], WV.at[st], ixs, ixr.at[st], (r, tp))

    def ix_start(d, _):
        ix_copy(d).start()
        return 0

    lax.fori_loop(1, NST, ix_start, 0)
    pltpu.make_async_copy(OV.at[st], WV.at[st], ixr.at[st]).start()

    def direct(t):
        s = seq_of(t)
        src = tokens.at[rows(s), :]
        dst = G.at[tp, rows(s), :]
        rcopy(src, dst, gsend, agr.at[t, 0], dev_y(1)).start()
        rcopy(src, dst, gsend, agr.at[t, 1], dev_y(-1)).start()
        rcopy(src, dst, gsend, sib.at[t, 0], sibling).start()

    def gblk(d):
        return ring(y, d) * 2 + k


    direct(0)
    direct(1)

    for c in loads[4:]:
        c.wait()

    def kv_body(i, _):
        store_copy(i).wait()
        r = pl.ds(pl.multiple_of(i * SEQ, SEQ), SEQ)
        kv = jnp.dot(ST[r, :], WKV[...], preferred_element_type=F32).astype(BF16)
        for j in range(4):
            TB[i * 4 + j] = kv[j * PLEN : (j + 1) * PLEN]
        return 0

    lax.fori_loop(0, 8, kv_body, 0)

    arrived(W.at[:, k, y], wloc.at[0])

    def w1_copy(dy):
        blk = W.at[st, k, y]
        return rcopy(blk, blk, wsend, w1.at[dy - 1], (st, lax.rem(y + dy, 4) * 2 + k))

    def w1_start(dy, _):
        w1_copy(dy).start()
        return 0

    lax.fori_loop(1, 4, w1_start, 0)
    rcopy(W.at[:, k, y], W.at[:, k, y], wsend, wsib.at[3], sibling).start()

    def send_kv():
        def w(r, _):
            arrived(WV.at[r], ixr.at[r])
            return 0

        lax.fori_loop(0, NST, w, 0)
        c = pltpu.make_async_copy(WV, WS, lsem.at[8])
        c.start()
        c.wait()

        def go(d, _):
            r = lax.rem(st + d, NST)
            for j in range(CAP):
                KS[r, j] = TB[WS[r, 0, j]]
            rcopy(KS.at[r], KR.at[pl.ds(st * CAP, CAP)], kvs, kvr.at[st], (r, tp)).start()
            return 0

        lax.fori_loop(1, NST, go, 0)
        for j in range(CAP):
            KS[st, j] = TB[WS[st, 0, j]]
        pltpu.make_async_copy(KS.at[st], KR.at[pl.ds(st * CAP, CAP)], kvr.at[st]).start()

    def dev_a(d):
        return (stidx(ring(a, d), b), tp)

    def dev_b(d):
        return (stidx(a, ring(b, d)), tp)

    def yo(dy):
        return lax.rem(y + dy, 4)

    def plane1():
        def go(dy, _):
            arrived(W.at[st, k, yo(4 - dy)], w1.at[dy - 1])
            return 0

        lax.fori_loop(1, 4, go, 0)

        def go2(j, _):
            da = lax.div(j, 3) + 1
            dy = lax.rem(j, 3) + 1
            blk = W.at[st, k, yo(dy)]
            rcopy(blk, blk, wsend, p1.at[j], (stidx(lax.rem(a + da, 4), b), tp)).start()
            return 0

        lax.fori_loop(0, 9, go2, 0)

    def plane2():
        def go(j, _):
            da = lax.div(j, 3) + 1
            dy = lax.rem(j, 3) + 1
            arrived(W.at[stidx(lax.rem(a + 4 - da, 4), b), k, yo(dy)], p1.at[j])
            return 0

        lax.fori_loop(0, 9, go, 0)

        def go2(j, _):
            blk = W.at[stidx(lax.div(j, 3), b), k, yo(lax.rem(j, 3) + 1)]
            rcopy(blk, blk, wsend, p2.at[0, j], dev_b(1)).start()
            rcopy(blk, blk, wsend, p2.at[1, j], dev_b(-1)).start()
            return 0

        lax.fori_loop(0, 12, go2, 0)

    def plane3():
        def blk(j, d):
            return W.at[stidx(lax.div(j, 3), ring(b, d)), k, yo(lax.rem(j, 3) + 1)]

        def go(j, _):
            arrived(blk(j, -1), p2.at[0, j])
            arrived(blk(j, 1), p2.at[1, j])
            return 0

        lax.fori_loop(0, 12, go, 0)

        def up(j, _):
            rcopy(blk(j, -1), blk(j, -1), wsend, p2.at[2, j], dev_b(1)).start()
            return 0

        def down(j, _):
            rcopy(blk(j, 1), blk(j, 1), wsend, p2.at[2, j], dev_b(-1)).start()
            return 0

        lax.fori_loop(0, 6, up, 0)
        lax.fori_loop(6, 12, down, 0)

    def plane4():
        def go(j, _):
            arrived(W.at[stidx(lax.div(j, 3), ring(b, 2)), k, yo(lax.rem(j, 3) + 1)], p2.at[2, j])
            return 0

        lax.fori_loop(0, 12, go, 0)

        def go2(dy, _):
            blk = W.at[:, k, yo(dy)]
            rcopy(blk, blk, wsend, wsib.at[dy - 1], sibling).start()
            return 0

        lax.fori_loop(1, 4, go2, 0)

    def send_branch(m, s):
        @pl.when(s != tp)
        def _():
            rcopy(AS.at[m, s], A.at[m, tp], asend, arecv.at[m, tp], (st, s)).start()

        @pl.when(s == tp)
        def _():
            pltpu.make_async_copy(AS.at[m, s], A.at[m, tp], arecv.at[m, tp]).start()

    for c in loads[:4]:
        c.wait()
    own.wait()
    rowf = lax.broadcasted_iota(jnp.int32, (SEQ, 128), 0)

    def gathered(s):
        r = rows(s)
        return jnp.concatenate([G[j, r, :] for j in range(NTP)], axis=1)

    def project(t):
        s = seq_of(t)

        def w(d):
            return G.at[ring(y, d) * 2 + (1 - k), rows(s), :]

        arrived(w(0), sib.at[t, 0])
        arrived(w(-1), sib.at[t, 1])
        arrived(w(1), sib.at[t, 2])
        arrived(w(2), sib.at[t, 3])
        p = jnp.dot(gathered(s), WIN[...], preferred_element_type=F32)
        Q[rows(s), :] = p[:, 0:128].astype(BF16)
        mixed = p[:, 256:384] * p[:, 384:512]
        tv = taps[...].astype(F32)
        m1 = jnp.where(rowf >= 1, pltpu.roll(mixed, 1, 0), 0.0)
        m2 = jnp.where(rowf >= 2, pltpu.roll(mixed, 2, 0), 0.0)
        filt = tv[0:1] * m2 + tv[1:2] * m1 + tv[2:3] * mixed
        AS[0, s] = (p[:, 128:256] * filt).astype(BF16)
        send_branch(0, s)

    HALF = SEQ // 2

    def step(t, _):
        @pl.when(t < 8)
        def _():
            s = seq_of(t)
            g = G.at[gblk(-1), rows(s), :]
            arrived(g, agr.at[t, 0])
            h = G.at[gblk(-1), rows(s, 0, HALF), :]
            rcopy(h, h, gsend, agr.at[t, 2], dev_y(1)).start()
            rcopy(g, g, gsend, sib.at[t, 1], sibling).start()
            g2 = G.at[gblk(1), rows(s), :]
            arrived(g2, agr.at[t, 1])
            h2 = G.at[gblk(1), rows(s, HALF, HALF), :]
            rcopy(h2, h2, gsend, agr.at[t, 3], dev_y(-1)).start()
            rcopy(g2, g2, gsend, sib.at[t, 2], sibling).start()

        @pl.when(t < 6)
        def _():
            direct(t + 2)

        @pl.when(t == 0)
        def _():
            send_kv()

        @pl.when(t == 1)
        def _():
            plane1()

        @pl.when(t == 3)
        def _():
            plane2()

        @pl.when(t == 6)
        def _():
            plane3()

        @pl.when((t >= 1) & (t < 9))
        def _():
            u = t - 1
            s = seq_of(u)
            arrived(G.at[gblk(2), rows(s, 0, HALF), :], agr.at[u, 2])
            arrived(G.at[gblk(2), rows(s, HALF, HALF), :], agr.at[u, 3])
            g = G.at[gblk(2), rows(s), :]
            rcopy(g, g, gsend, sib.at[u, 3], sibling).start()

        @pl.when(t >= 2)
        def _():
            project(t - 2)

        return 0

    lax.fori_loop(0, 10, step, 0)
    plane4()

    def wkv(r, _):
        arrived(KR.at[pl.ds(r * CAP, CAP)], kvr.at[r])
        return 0

    lax.fori_loop(0, NST, wkv, 0)
    pcopy.wait()

    def attend(t, _):
        s = seq_of(t)
        for h in range(2):
            n = (s * 2 + h) * 2
            kv = jnp.concatenate([KR[PS[n, 0, 0]], KR[PS[n + 1, 0, 0]]], axis=0)
            q = Q[rows(s, h * BLOCK, BLOCK), :]
            sc = lax.dot_general(
                q, kv[:, :128], (((1,), (1,)), ((), ())), preferred_element_type=F32
            ) * (HEAD_SIZE ** -0.5)
            e = jnp.exp(sc - jnp.max(sc, axis=1, keepdims=True))
            wt = (e / jnp.sum(e, axis=1, keepdims=True)).astype(BF16)
            o = jnp.dot(wt, kv[:, 128:], preferred_element_type=F32)
            AS[1, s, pl.ds(h * BLOCK, BLOCK), :] = o.astype(BF16)
        send_branch(1, s)
        return 0

    lax.fori_loop(0, 8, attend, 0)

    logits = lax.dot_general(
        gathered(tp), route[...], (((1,), (1,)), ((), ())), preferred_element_type=F32
    )
    mix = jax.nn.sigmoid(logits)
    mix0 = mix[:, 0:1]
    mix1 = mix[:, 1:2]

    def wa(j, _):
        arrived(A.at[0, j], arecv.at[0, j])
        arrived(A.at[1, j], arecv.at[1, j])
        return 0

    lax.fori_loop(0, NTP, wa, 0)

    def wws(dy, _):
        arrived(W.at[:, 1 - k, yo(dy)], wsib.at[lax.rem(dy + 3, 4)])
        return 0

    lax.fori_loop(0, 4, wws, 0)

    order = [(kk, yy) for kk in range(2) for yy in range(4)]

    def outp(c, _):
        acc = []
        for m in range(2):
            lhs = jnp.concatenate([A[m, yy * 2 + kk] for kk, yy in order], axis=1)
            rhs = jnp.concatenate(
                [
                    jnp.concatenate([W[c * 2 + h, kk, yy, m] for kk, yy in order], axis=0)
                    for h in range(2)
                ],
                axis=1,
            )
            acc.append(jnp.dot(lhs, rhs, preferred_element_type=F32))
        out[:, pl.ds(pl.multiple_of(c * 256, 256), 256)] = (mix0 * acc[0] + mix1 * acc[1]).astype(BF16)
        return 0

    lax.fori_loop(0, 8, outp, 0)

    arrived(OV.at[pl.ds(0, NST - 1)], ixs)
    arrived(KS.at[pl.ds(0, NST - 1)], kvs)
    arrived(G.at[pl.ds(0, 7)], gsend)
    arrived(AS.at[:, pl.ds(0, 7)], asend)
    arrived(W.at[pl.ds(0, 14)], wsend)


def local(
    tokens, store, holder, slot, wq, wk, wval, wo, wi, wv, taps, route, cout, mout
):
    anyspec = pl.BlockSpec(memory_space=pl.ANY)
    vmem = pl.BlockSpec(memory_space=pltpu.VMEM)
    smem = pl.BlockSpec(memory_space=pltpu.SMEM)
    dma = pltpu.SemaphoreType.DMA
    V = pltpu.VMEM
    return pl.pallas_call(
        kernel,
        out_shape=jax.ShapeDtypeStruct((SEQ, cout.shape[1]), BF16),
        in_specs=[anyspec, anyspec, smem, smem] + [anyspec] * 6 + [vmem, vmem, anyspec, anyspec],
        out_specs=vmem,
        scratch_shapes=[
            V((8, 2048, 256), BF16),
            V((2048, 2048), BF16),
            V((2048, 512), BF16),
            V((2048, 256), BF16),
            V((32, PLEN, 256), BF16),
            V((NST, CAP, PLEN, 256), BF16),
            V((NST * CAP, PLEN, 256), BF16),
            V((NST, 1, 128), jnp.int32),
            V((NST, 1, 128), jnp.int32),
            pltpu.SMEM((NST, 1, 128), jnp.int32),
            V((32, 1, 128), jnp.int32),
            pltpu.SMEM((32, 1, 128), jnp.int32),
            V((2048, 128), BF16),
            V((2, 8, SEQ, 128), BF16),
            V((2, 8, SEQ, 128), BF16),
            V((NST, 2, 4, 2, 128, 128), BF16),
            dma((9,)), dma((8,)), dma((NST,)), dma, dma((NST,)), dma,
            dma((8, 4)), dma((8, 4)), dma, dma((2, 8)), dma,
            dma((1,)), dma((3,)), dma((9,)), dma((3, 12)), dma((4,)), dma,
        ],
        compiler_params=pltpu.CompilerParams(
            collective_id=0, has_side_effects=True, vmem_limit_bytes=60 * 1024 * 1024
        ),
    )(
        tokens, store.reshape(-1, store.shape[-1]), holder.T, slot.T,
        wq, wo, wi, wv, wk, wval, taps, route.T, cout, mout,
    )


def solution(mesh):
    return jax.shard_map(
        local,
        mesh=mesh,
        in_specs=(
            P("st", "tp"), P("st", None, None), P("st", None), P("st", None),
            P(None, "tp"), P(None, "tp"), P(None, "tp"), P(None, "tp"), P(None, "tp"),
            P(None, "tp"), P(None, "tp"), P(), P("tp", None), P("tp", None),
        ),
        out_specs=P(("st", "tp"), None),
        check_vma=False,
    )
```

time: 160 us -> 87 us (0.54)
  Pallas kernels: 0 us -> 84.5 us
  waiting for transfers between devices: 81.2 us -> 0 us
  matrix products: 35.3 us -> 0 us
  starting transfers between devices: 15.4 us -> 0 us
  between operations: 13.7 us -> 0.01 us
  local copies, waits for them, and re-layouts: 10.7 us -> 2.3 us
  other arithmetic: 3.89 us -> 0 us
    pallas_call x0 -> x1, Pallas kernels: none -> 84.5 us  [local(): pl.pallas_call(kernel, out_shape=jax.ShapeDtypeStruct((SEQ, cout.shape[1]...]
    reduce_scatter x1 -> x0, waiting for transfers between devices: 52.1 us -> none  [local(): lax.psum_scatter((branch_mix[:, 0:1] * jnp.dot(conv_branch, conv_out, pre...]
    dot_general x8 -> x0, matrix products: 34.7 us -> none  [the longest x1 7.57 us: local(): jnp.dot(pieces, local_weight, preferred_element_type=jnp.float32)]
    all_to_all x2 -> x0, waiting for transfers between devices: 28.3 us -> none  [the longest x1 28.3 us: local(): lax.all_to_all(chosen, 'st', split_axis=0, concat_axis=0, tiled=True)]
    all_to_all x2 -> x0, starting transfers between devices: 15.2 us -> none  [the longest x1 8.42 us: local(): lax.all_to_all(outgoing, 'st', split_axis=0, concat_axis=0, tiled=True)]
    gather x2 -> x0, local copies, waits for them, and re-layouts: 3.65 us -> none  [the longest x1 2.07 us: local(): chosen = table[wanted.reshape(-1)].reshape(wanted.shape + table.shape[1:])]
    unnamed x24 -> x1, local copies, waits for them, and re-layouts: 4.49 us -> 2.3 us
    mul x2 -> x0, other arithmetic: 1.66 us -> none  [the longest x1 1.65 us: local(): inner_part * value_part]
  transfers between devices with their start and end apart: 4 -> 0, of which waited for: 2 -> 0; matrix products, arithmetic and copies ran while one was open for 11% -> 0% of each run, Pallas kernels for 0% -> 0%
where the time goes in v1:
time: 87 us; the launch traced here: 86.8 us
  Pallas kernels  84.5 us (97%)
  local copies, waits for them, and re-layouts  2.3 us (3%)
    pallas_call x1, Pallas kernels, local(): pl.pallas_call(kernel, out_shape=jax.ShapeDtypeStruct((SEQ, cout.shape[1]...  84.5 us
    unnamed x1, local copies, waits for them, and re-layouts  2.3 us

profile of v1, /device:TPU:1, one launch (start us, length us, event | category | flops | bytes accessed | tf_op | source)
XLA Modules:
  0.0 86.8 jit_solution(4964318287089467023)
XLA Ops:
  0.0 84.5 %shard_map.136 = bf16[256,2048]{1,0:T(8,128)(2,1)} custom-call(bf16[2048,256]{1,0:T(8,128)(2,1)} %tokens.1, bf16[2048,2048]{1,0:T(8,128)(2,1)} %bitcast.4, s32[2,16]{1,0:T(2,128)} %bitcast.6, s32[2,16]{1,0:T(2,128)} %bitcast.7, bf16[2048,128]{1,0:T(8,128)(2,1)} %wq.1, bf16[2048,128]{1,0:T(8,128)(2,1)} %wo.1, bf16[2048,128]{1,0:T(8,128)(2,1)} %wi.1, ...), custom_call_target="tpu_custom_call" | custom-call | tf_op jit(solution)/shard_map/pallas_call | solution.py:454
  84.5 2.3 %copy.16 = bf16[256,2048]{1,0:T(8,128)(2,1)} copy(bf16[256,2048]{1,0:T(8,128)(2,1)} %shard_map.136) | data formatting | bytes 2097152

commit v2 on v1

--- a/solution.py
+++ b/solution.py
@@ -20,11 +20,11 @@
 
 
 def kernel(
-    tokens, store, holder, slot, wq, wo, wi, wv, wk, wval, taps, route, cout, mout,
+    tokens, store, holder_h, slot_h, wq, wo, wi, wv, wk, wval, taps_h, route_h, cout, mout,
     out,
-    G, ST, WIN, WKV, TB, KS, KR, OV, WV, WS, PV, PS, Q, AS, A, W,
+    holder, slot, taps, route, G, ST, WIN, WKV, TB, KS, KR, OV, WV, WS, PV, PS, Q, AS, A, W,
     lsem, stsem, ixr, ixs, kvr, kvs, agr, sib, gsend, arecv, asend,
-    wloc, w1, p1, p2, wsib, wsend,
+    wloc, w1, p1, p2, wsib, wsown, wsend,
 ):
     st = lax.axis_index("st")
     tp = lax.axis_index("tp")
@@ -61,13 +61,30 @@
     def rows(s, lo=0, n=SEQ):
         return pl.ds(pl.multiple_of(s * SEQ + lo, 64), n)
 
+    bar = pltpu.get_barrier_semaphore()
+
+    def sig_tp(d, _):
+        pl.semaphore_signal(bar, inc=1, device_id=(st, lax.rem(tp + d, NTP)), device_id_type=MESH)
+        return 0
+
+    def sig_st(d, _):
+        pl.semaphore_signal(bar, inc=1, device_id=(lax.rem(st + d, NST), tp), device_id_type=MESH)
+        return 0
+
+    lax.fori_loop(1, NTP, sig_tp, 0)
+    lax.fori_loop(1, NST, sig_st, 0)
+
     loads = []
     for j, w in enumerate((wq, wo, wi, wv)):
         loads.append(pltpu.make_async_copy(w, WIN.at[:, pl.ds(j * 128, 128)], lsem.at[j]))
     for j, w in enumerate((wk, wval)):
         loads.append(pltpu.make_async_copy(w, WKV.at[:, pl.ds(j * 128, 128)], lsem.at[4 + j]))
     own = pltpu.make_async_copy(tokens, G.at[tp], lsem.at[6])
-    for c in loads[4:]:
+    small = [
+        pltpu.make_async_copy(p, q, lsem.at[9 + j])
+        for j, (p, q) in enumerate(((holder_h, holder), (slot_h, slot), (taps_h, taps), (route_h, route)))
+    ]
+    for c in small + loads[4:]:
         c.start()
 
     def store_copy(i):
@@ -83,31 +100,17 @@
         c.start()
     own.start()
 
-    def wl(cs, m):
-        src = (cout, mout)[m]
-        return pltpu.make_async_copy(
-            src.at[:, pl.ds(pl.multiple_of(cs * 128, 128), 128)], W.at[cs, k, y, m], wloc.at[0]
-        )
+    def wcol(m, cs):
+        return (cout, mout)[m].at[:, pl.ds(pl.multiple_of(cs * 128, 128), 128)]
 
     def start_wl(cs, _):
-        wl(cs, 0).start()
-        wl(cs, 1).start()
+        for m in range(2):
+            pltpu.make_async_copy(wcol(m, cs), W.at[cs, k, y, m], wloc.at[0]).start()
         return 0
 
     lax.fori_loop(0, NST, start_wl, 0)
-
-    bar = pltpu.get_barrier_semaphore()
-
-    def sig_tp(d, _):
-        pl.semaphore_signal(bar, inc=1, device_id=(st, lax.rem(tp + d, NTP)), device_id_type=MESH)
-        return 0
-
-    def sig_st(d, _):
-        pl.semaphore_signal(bar, inc=1, device_id=(lax.rem(st + d, NST), tp), device_id_type=MESH)
-        return 0
-
-    lax.fori_loop(1, NTP, sig_tp, 0)
-    lax.fori_loop(1, NST, sig_st, 0)
+    for c in small[:2]:
+        c.wait()
 
     rowi = lax.broadcasted_iota(jnp.int32, (NST, 128), 0)
     lanei = lax.broadcasted_iota(jnp.int32, (NST, 128), 1)
@@ -151,6 +154,16 @@
 
 
     direct(0)
+
+    def w1_start(dy, _):
+        for m in range(2):
+            rcopy(
+                wcol(m, st), W.at[st, k, y, m], wsend, w1.at[(dy - 1) * 2 + m],
+                (st, lax.rem(y + dy, 4) * 2 + k),
+            ).start()
+        return 0
+
+    lax.fori_loop(1, 4, w1_start, 0)
     direct(1)
 
     for c in loads[4:]:
@@ -166,19 +179,6 @@
 
     lax.fori_loop(0, 8, kv_body, 0)
 
-    arrived(W.at[:, k, y], wloc.at[0])
-
-    def w1_copy(dy):
-        blk = W.at[st, k, y]
-        return rcopy(blk, blk, wsend, w1.at[dy - 1], (st, lax.rem(y + dy, 4) * 2 + k))
-
-    def w1_start(dy, _):
-        w1_copy(dy).start()
-        return 0
-
-    lax.fori_loop(1, 4, w1_start, 0)
-    rcopy(W.at[:, k, y], W.at[:, k, y], wsend, wsib.at[3], sibling).start()
-
     def send_kv():
         def w(r, _):
             arrived(WV.at[r], ixr.at[r])
@@ -212,7 +212,8 @@
 
     def plane1():
         def go(dy, _):
-            arrived(W.at[st, k, yo(4 - dy)], w1.at[dy - 1])
+            for m in range(2):
+                arrived(W.at[st, k, yo(4 - dy), m], w1.at[(dy - 1) * 2 + m])
             return 0
 
         lax.fori_loop(1, 4, go, 0)
@@ -243,41 +244,37 @@
 
         lax.fori_loop(0, 12, go2, 0)
 
+    def wblk(j, d):
+        return W.at[stidx(lax.div(j, 3), ring(b, d)), k, yo(lax.rem(j, 3) + 1)]
+
+    def wpass(lo, hi, d, sem, dev):
+        def go(j, _):
+            g = wblk(j, d)
+            rcopy(g, g, wsend, sem.at[j], dev).start()
+            return 0
+
+        lax.fori_loop(lo, hi, go, 0)
+
     def plane3():
-        def blk(j, d):
-            return W.at[stidx(lax.div(j, 3), ring(b, d)), k, yo(lax.rem(j, 3) + 1)]
-
         def go(j, _):
-            arrived(blk(j, -1), p2.at[0, j])
-            arrived(blk(j, 1), p2.at[1, j])
+            arrived(wblk(j, -1), p2.at[0, j])
+            arrived(wblk(j, 1), p2.at[1, j])
             return 0
 
         lax.fori_loop(0, 12, go, 0)
-
-        def up(j, _):
-            rcopy(blk(j, -1), blk(j, -1), wsend, p2.at[2, j], dev_b(1)).start()
-            return 0
-
-        def down(j, _):
-            rcopy(blk(j, 1), blk(j, 1), wsend, p2.at[2, j], dev_b(-1)).start()
-            return 0
-
-        lax.fori_loop(0, 6, up, 0)
-        lax.fori_loop(6, 12, down, 0)
+        wpass(0, 6, -1, p2.at[2], dev_b(1))
+        wpass(6, 12, 1, p2.at[2], dev_b(-1))
+        wpass(0, 12, 0, wsib.at[0], sibling)
+        wpass(0, 12, 1, wsib.at[1], sibling)
+        wpass(0, 12, -1, wsib.at[3], sibling)
 
     def plane4():
         def go(j, _):
-            arrived(W.at[stidx(lax.div(j, 3), ring(b, 2)), k, yo(lax.rem(j, 3) + 1)], p2.at[2, j])
+            arrived(wblk(j, 2), p2.at[2, j])
             return 0
 
         lax.fori_loop(0, 12, go, 0)
-
-        def go2(dy, _):
-            blk = W.at[:, k, yo(dy)]
-            rcopy(blk, blk, wsend, wsib.at[dy - 1], sibling).start()
-            return 0
-
-        lax.fori_loop(1, 4, go2, 0)
+        wpass(0, 12, 2, wsib.at[2], sibling)
 
     def send_branch(m, s):
         @pl.when(s != tp)
@@ -288,9 +285,11 @@
         def _():
             pltpu.make_async_copy(AS.at[m, s], A.at[m, tp], arecv.at[m, tp]).start()
 
-    for c in loads[:4]:
+    for c in loads[:4] + small[2:]:
         c.wait()
     own.wait()
+    arrived(W.at[:, k, y], wloc.at[0])
+    rcopy(W.at[:, k, y], W.at[:, k, y], wsend, wsown.at[0], sibling).start()
     rowf = lax.broadcasted_iota(jnp.int32, (SEQ, 128), 0)
 
     def gathered(s):
@@ -317,6 +316,35 @@
         AS[0, s] = (p[:, 128:256] * filt).astype(BF16)
         send_branch(0, s)
 
+    def wkv(r, _):
+        arrived(KR.at[pl.ds(r * CAP, CAP)], kvr.at[r])
+        return 0
+
+    def attend(ts):
+        parts = [(seq_of(t), h) for t in ts for h in range(2)]
+        kvs_, sc = [], []
+        for s, h in parts:
+            n = (s * 2 + h) * 2
+            kv = jnp.concatenate([KR[PS[n, 0, 0]], KR[PS[n + 1, 0, 0]]], axis=0)
+            q = Q[rows(s, h * BLOCK, BLOCK), :]
+            kvs_.append(kv)
+            sc.append(
+                lax.dot_general(
+                    q, kv[:, :128], (((1,), (1,)), ((), ())), preferred_element_type=F32
+                ) * (HEAD_SIZE ** -0.5)
+            )
+        e = [jnp.exp(v - jnp.max(v, axis=1, keepdims=True)) for v in sc]
+        wt = [(v / jnp.sum(v, axis=1, keepdims=True)).astype(BF16) for v in e]
+        for (s, h), kv, v in zip(parts, kvs_, wt):
+            o = jnp.dot(v, kv[:, 128:], preferred_element_type=F32)
+            AS[1, s, pl.ds(h * BLOCK, BLOCK), :] = o.astype(BF16)
+        for t in ts:
+            send_branch(1, seq_of(t))
+
+    def attend2(i, _):
+        attend([2 * i, 2 * i + 1])
+        return 0
+
     HALF = SEQ // 2
 
     def step(t, _):
@@ -340,19 +368,12 @@
 
         @pl.when(t == 0)
         def _():
+            plane1()
             send_kv()
 
-        @pl.when(t == 1)
-        def _():
-            plane1()
-
-        @pl.when(t == 3)
+        @pl.when(t == 2)
         def _():
             plane2()
-
-        @pl.when(t == 6)
-        def _():
-            plane3()
 
         @pl.when((t >= 1) & (t < 9))
         def _():
@@ -367,35 +388,27 @@
         def _():
             project(t - 2)
 
+        @pl.when(t == 6)
+        def _():
+            lax.fori_loop(0, NST, wkv, 0)
+            pcopy.wait()
+
+        @pl.when((t == 6) | (t == 7))
+        def _():
+            lax.fori_loop((t - 6) * 2, t - 4, attend2, 0)
+
+        @pl.when(t >= 8)
+        def _():
+            attend([t - 2])
+
+        @pl.when(t == 8)
+        def _():
+            plane3()
+
         return 0
 
     lax.fori_loop(0, 10, step, 0)
     plane4()
-
-    def wkv(r, _):
-        arrived(KR.at[pl.ds(r * CAP, CAP)], kvr.at[r])
-        return 0
-
-    lax.fori_loop(0, NST, wkv, 0)
-    pcopy.wait()
-
-    def attend(t, _):
-        s = seq_of(t)
-        for h in range(2):
-            n = (s * 2 + h) * 2
-            kv = jnp.concatenate([KR[PS[n, 0, 0]], KR[PS[n + 1, 0, 0]]], axis=0)
-            q = Q[rows(s, h * BLOCK, BLOCK), :]
-            sc = lax.dot_general(
-                q, kv[:, :128], (((1,), (1,)), ((), ())), preferred_element_type=F32
-            ) * (HEAD_SIZE ** -0.5)
-            e = jnp.exp(sc - jnp.max(sc, axis=1, keepdims=True))
-            wt = (e / jnp.sum(e, axis=1, keepdims=True)).astype(BF16)
-            o = jnp.dot(wt, kv[:, 128:], preferred_element_type=F32)
-            AS[1, s, pl.ds(h * BLOCK, BLOCK), :] = o.astype(BF16)
-        send_branch(1, s)
-        return 0
-
-    lax.fori_loop(0, 8, attend, 0)
 
     logits = lax.dot_general(
         gathered(tp), route[...], (((1,), (1,)), ((), ())), preferred_element_type=F32
@@ -411,11 +424,16 @@
 
     lax.fori_loop(0, NTP, wa, 0)
 
-    def wws(dy, _):
-        arrived(W.at[:, 1 - k, yo(dy)], wsib.at[lax.rem(dy + 3, 4)])
-        return 0
-
-    lax.fori_loop(0, 4, wws, 0)
+    def wws(j, _):
+        for d in range(4):
+            bs = lax.rem((1 - k) * x + k * z + d, 4)
+            i = lax.div(j, 3)
+            blk = (1 - k) * (i * NXZ + bs) + k * (bs * NXZ + i)
+            arrived(W.at[blk, 1 - k, yo(lax.rem(j, 3) + 1)], wsib.at[d, j])
+        return 0
+
+    arrived(W.at[:, 1 - k, y], wsown.at[0])
+    lax.fori_loop(0, 12, wws, 0)
 
     order = [(kk, yy) for kk in range(2) for yy in range(4)]
 
@@ -446,17 +464,20 @@
 def local(
     tokens, store, holder, slot, wq, wk, wval, wo, wi, wv, taps, route, cout, mout
 ):
-    anyspec = pl.BlockSpec(memory_space=pl.ANY)
+    hbm = pl.BlockSpec(memory_space=pltpu.HBM)
     vmem = pl.BlockSpec(memory_space=pltpu.VMEM)
-    smem = pl.BlockSpec(memory_space=pltpu.SMEM)
     dma = pltpu.SemaphoreType.DMA
     V = pltpu.VMEM
     return pl.pallas_call(
         kernel,
         out_shape=jax.ShapeDtypeStruct((SEQ, cout.shape[1]), BF16),
-        in_specs=[anyspec, anyspec, smem, smem] + [anyspec] * 6 + [vmem, vmem, anyspec, anyspec],
+        in_specs=[hbm] * 14,
         out_specs=vmem,
         scratch_shapes=[
+            pltpu.SMEM((2, 16), jnp.int32),
+            pltpu.SMEM((2, 16), jnp.int32),
+            V((3, 128), BF16),
+            V((2, 2048), BF16),
             V((8, 2048, 256), BF16),
             V((2048, 2048), BF16),
             V((2048, 512), BF16),
@@ -473,16 +494,21 @@
             V((2, 8, SEQ, 128), BF16),
             V((2, 8, SEQ, 128), BF16),
             V((NST, 2, 4, 2, 128, 128), BF16),
-            dma((9,)), dma((8,)), dma((NST,)), dma, dma((NST,)), dma,
+            dma((13,)), dma((8,)), dma((NST,)), dma, dma((NST,)), dma,
             dma((8, 4)), dma((8, 4)), dma, dma((2, 8)), dma,
-            dma((1,)), dma((3,)), dma((9,)), dma((3, 12)), dma((4,)), dma,
+            dma((1,)), dma((6,)), dma((9,)), dma((3, 12)), dma((4, 12)), dma((1,)), dma,
         ],
         compiler_params=pltpu.CompilerParams(
-            collective_id=0, has_side_effects=True, vmem_limit_bytes=60 * 1024 * 1024
+            collective_id=0, has_side_effects=True, vmem_limit_bytes=44 * 1024 * 1024
         ),
     )(
-        tokens, store.reshape(-1, store.shape[-1]), holder.T, slot.T,
-        wq, wo, wi, wv, wk, wval, taps, route.T, cout, mout,
+        *(
+            pltpu.with_memory_space_constraint(v, pltpu.HBM)
+            for v in (
+                tokens, store.reshape(-1, store.shape[-1]), holder.T, slot.T,
+                wq, wo, wi, wv, wk, wval, taps, route.T, cout, mout,
+            )
+        )
     )
 
 

time: 87 us -> 79.2 us (0.910)
  the two profiles are of different devices: /device:TPU:1 before, /device:TPU:25 now
where the time goes in v2:
time: 79.2 us; the launch traced here: 79.1 us
  Pallas kernels  78.2 us (99%)
  local copies, waits for them, and re-layouts  0.97 us (1%)
    pallas_call x1, Pallas kernels, local(): pl.pallas_call(kernel, out_shape=jax.ShapeDtypeStruct((SEQ, cout.shape[1]...  78.2 us

profile of v2, /device:TPU:25, one launch (start us, length us, event | category | flops | bytes accessed | tf_op | source)
XLA Modules:
  0.0 79.1 jit_solution(8165226789178087956)
XLA Ops:
  0.0 78.2 %shard_map.136 = bf16[256,2048]{1,0:T(8,128)(2,1)S(1)} custom-call(bf16[2048,256]{1,0:T(8,128)(2,1)} %tokens.1, bf16[2048,2048]{1,0:T(8,128)(2,1)} %bitcast.4, s32[2,16]{1,0:T(2,128)} %bitcast.6, s32[2,16]{1,0:T(2,128)} %bitcast.7, bf16[2048,128]{1,0:T(8,128)(2,1)} %wq.1, bf16[2048,128]{1,0:T(8,128)(2,1)} %wo.1, bf16[2048,128]{1,0:T(8,128)(2,1)} %wi.1, ...), custom_call_target="tpu_custom_call" | custom-call | tf_op jit(solution)/shard_map/pallas_call | solution.py:471
  78.2 1.0 %copy.16 = bf16[256,2048]{1,0:T(8,128)(2,1)} copy(bf16[256,2048]{1,0:T(8,128)(2,1)S(1)} %shard_map.136) | data formatting | bytes 2097152

commit v3 on v2

--- a/solution.py
+++ b/solution.py
@@ -22,9 +22,9 @@
 def kernel(
     tokens, store, holder_h, slot_h, wq, wo, wi, wv, wk, wval, taps_h, route_h, cout, mout,
     out,
-    holder, slot, taps, route, G, ST, WIN, WKV, TB, KS, KR, OV, WV, WS, PV, PS, Q, AS, A, W,
+    OB, holder, slot, taps, route, G, ST, WIN, WKV, TB, KS, KR, OV, WV, WS, PV, PS, Q, AS, A, W,
     lsem, stsem, ixr, ixs, kvr, kvs, agr, sib, gsend, arecv, asend,
-    wloc, w1, p1, p2, wsib, wsown, wsend,
+    wloc, w1, p1, p2, wsib, wsown, wsend, osem,
 ):
     st = lax.axis_index("st")
     tp = lax.axis_index("tp")
@@ -76,12 +76,12 @@
 
     loads = []
     for j, w in enumerate((wq, wo, wi, wv)):
-        loads.append(pltpu.make_async_copy(w, WIN.at[:, pl.ds(j * 128, 128)], lsem.at[j]))
+        loads.append(pltpu.make_async_copy(w, WIN.at[:, pl.ds(j * 128, 128)], lsem.at[0]))
     for j, w in enumerate((wk, wval)):
-        loads.append(pltpu.make_async_copy(w, WKV.at[:, pl.ds(j * 128, 128)], lsem.at[4 + j]))
-    own = pltpu.make_async_copy(tokens, G.at[tp], lsem.at[6])
+        loads.append(pltpu.make_async_copy(w, WKV.at[:, pl.ds(j * 128, 128)], lsem.at[1]))
+    own = pltpu.make_async_copy(tokens, G.at[tp], lsem.at[2])
     small = [
-        pltpu.make_async_copy(p, q, lsem.at[9 + j])
+        pltpu.make_async_copy(p, q, lsem.at[3 + j])
         for j, (p, q) in enumerate(((holder_h, holder), (slot_h, slot), (taps_h, taps), (route_h, route)))
     ]
     for c in small + loads[4:]:
@@ -105,7 +105,7 @@
 
     def start_wl(cs, _):
         for m in range(2):
-            pltpu.make_async_copy(wcol(m, cs), W.at[cs, k, y, m], wloc.at[0]).start()
+            pltpu.make_async_copy(wcol(m, cs), W.at[cs, k, y, m], wloc).start()
         return 0
 
     lax.fori_loop(0, NST, start_wl, 0)
@@ -132,14 +132,14 @@
 
     def ix_copy(d):
         r = lax.rem(st + d, NST)
-        return rcopy(OV.at[r], WV.at[st], ixs, ixr.at[st], (r, tp))
+        return rcopy(OV.at[r], WV.at[st], ixs, ixr, (r, tp))
 
     def ix_start(d, _):
         ix_copy(d).start()
         return 0
 
     lax.fori_loop(1, NST, ix_start, 0)
-    pltpu.make_async_copy(OV.at[st], WV.at[st], ixr.at[st]).start()
+    pltpu.make_async_copy(OV.at[st], WV.at[st], ixr).start()
 
     def direct(t):
         s = seq_of(t)
@@ -147,27 +147,25 @@
         dst = G.at[tp, rows(s), :]
         rcopy(src, dst, gsend, agr.at[t, 0], dev_y(1)).start()
         rcopy(src, dst, gsend, agr.at[t, 1], dev_y(-1)).start()
-        rcopy(src, dst, gsend, sib.at[t, 0], sibling).start()
+        rcopy(src, dst, gsend, sib.at[t], sibling).start()
 
     def gblk(d):
         return ring(y, d) * 2 + k
 
-
-    direct(0)
 
     def w1_start(dy, _):
         for m in range(2):
             rcopy(
-                wcol(m, st), W.at[st, k, y, m], wsend, w1.at[(dy - 1) * 2 + m],
+                wcol(m, st), W.at[st, k, y, m], wsend, w1,
                 (st, lax.rem(y + dy, 4) * 2 + k),
             ).start()
         return 0
 
     lax.fori_loop(1, 4, w1_start, 0)
+    direct(0)
     direct(1)
 
-    for c in loads[4:]:
-        c.wait()
+    arrived(WKV, lsem.at[1])
 
     def kv_body(i, _):
         store_copy(i).wait()
@@ -180,26 +178,21 @@
     lax.fori_loop(0, 8, kv_body, 0)
 
     def send_kv():
-        def w(r, _):
-            arrived(WV.at[r], ixr.at[r])
-            return 0
-
-        lax.fori_loop(0, NST, w, 0)
-        c = pltpu.make_async_copy(WV, WS, lsem.at[8])
+        arrived(WV, ixr)
+        c = pltpu.make_async_copy(WV, WS, lsem.at[3])
         c.start()
         c.wait()
-
-        def go(d, _):
-            r = lax.rem(st + d, NST)
-            for j in range(CAP):
-                KS[r, j] = TB[WS[r, 0, j]]
-            rcopy(KS.at[r], KR.at[pl.ds(st * CAP, CAP)], kvs, kvr.at[st], (r, tp)).start()
-            return 0
-
-        lax.fori_loop(1, NST, go, 0)
+        lax.fori_loop(1, NST, kv_out, 0)
         for j in range(CAP):
             KS[st, j] = TB[WS[st, 0, j]]
-        pltpu.make_async_copy(KS.at[st], KR.at[pl.ds(st * CAP, CAP)], kvr.at[st]).start()
+        pltpu.make_async_copy(KS.at[st], KR.at[pl.ds(st * CAP, CAP)], kvr).start()
+
+    def kv_out(d, _):
+        r = lax.rem(st + d, NST)
+        for j in range(CAP):
+            KS[r, j] = TB[WS[r, 0, j]]
+        rcopy(KS.at[r], KR.at[pl.ds(st * CAP, CAP)], kvs, kvr, (r, tp)).start()
+        return 0
 
     def dev_a(d):
         return (stidx(ring(a, d), b), tp)
@@ -211,85 +204,71 @@
         return lax.rem(y + dy, 4)
 
     def plane1():
-        def go(dy, _):
-            for m in range(2):
-                arrived(W.at[st, k, yo(4 - dy), m], w1.at[(dy - 1) * 2 + m])
-            return 0
-
-        lax.fori_loop(1, 4, go, 0)
+        arrived(W.at[pl.ds(0, 3), 0, 0], w1)
 
         def go2(j, _):
             da = lax.div(j, 3) + 1
             dy = lax.rem(j, 3) + 1
             blk = W.at[st, k, yo(dy)]
-            rcopy(blk, blk, wsend, p1.at[j], (stidx(lax.rem(a + da, 4), b), tp)).start()
+            rcopy(blk, blk, wsend, p1, (stidx(lax.rem(a + da, 4), b), tp)).start()
             return 0
 
         lax.fori_loop(0, 9, go2, 0)
-
-    def plane2():
-        def go(j, _):
-            da = lax.div(j, 3) + 1
-            dy = lax.rem(j, 3) + 1
-            arrived(W.at[stidx(lax.rem(a + 4 - da, 4), b), k, yo(dy)], p1.at[j])
-            return 0
-
-        lax.fori_loop(0, 9, go, 0)
-
-        def go2(j, _):
-            blk = W.at[stidx(lax.div(j, 3), b), k, yo(lax.rem(j, 3) + 1)]
-            rcopy(blk, blk, wsend, p2.at[0, j], dev_b(1)).start()
-            rcopy(blk, blk, wsend, p2.at[1, j], dev_b(-1)).start()
-            return 0
-
-        lax.fori_loop(0, 12, go2, 0)
 
     def wblk(j, d):
         return W.at[stidx(lax.div(j, 3), ring(b, d)), k, yo(lax.rem(j, 3) + 1)]
 
-    def wpass(lo, hi, d, sem, dev):
+    def wpass(d, sem, dev):
         def go(j, _):
             g = wblk(j, d)
-            rcopy(g, g, wsend, sem.at[j], dev).start()
+            rcopy(g, g, wsend, sem, dev).start()
             return 0
 
-        lax.fori_loop(lo, hi, go, 0)
+        lax.fori_loop(0, 12, go, 0)
+
+    TWELVE = W.at[pl.ds(0, 3), 0]
+
+    def plane2():
+        arrived(W.at[pl.ds(0, 9), 0, 0], p1)
+
+        def go(j, _):
+            g = wblk(j, 0)
+            rcopy(g, g, wsend, p2.at[0], dev_b(1)).start()
+            rcopy(g, g, wsend, p2.at[1], dev_b(-1)).start()
+            return 0
+
+        lax.fori_loop(0, 12, go, 0)
+        wpass(0, p2.at[2], dev_b(2))
+        wpass(0, wsib.at[0], sibling)
 
     def plane3():
-        def go(j, _):
-            arrived(wblk(j, -1), p2.at[0, j])
-            arrived(wblk(j, 1), p2.at[1, j])
-            return 0
-
-        lax.fori_loop(0, 12, go, 0)
-        wpass(0, 6, -1, p2.at[2], dev_b(1))
-        wpass(6, 12, 1, p2.at[2], dev_b(-1))
-        wpass(0, 12, 0, wsib.at[0], sibling)
-        wpass(0, 12, 1, wsib.at[1], sibling)
-        wpass(0, 12, -1, wsib.at[3], sibling)
+        arrived(TWELVE, p2.at[0])
+        wpass(-1, wsib.at[1], sibling)
+        arrived(TWELVE, p2.at[1])
+        wpass(1, wsib.at[2], sibling)
 
     def plane4():
-        def go(j, _):
-            arrived(wblk(j, 2), p2.at[2, j])
-            return 0
-
-        lax.fori_loop(0, 12, go, 0)
-        wpass(0, 12, 2, wsib.at[2], sibling)
+        arrived(TWELVE, p2.at[2])
+        wpass(2, wsib.at[3], sibling)
+
+    plane1()
+    send_kv()
 
     def send_branch(m, s):
         @pl.when(s != tp)
         def _():
-            rcopy(AS.at[m, s], A.at[m, tp], asend, arecv.at[m, tp], (st, s)).start()
+            rcopy(AS.at[m, s], A.at[m, tp], asend, arecv, (st, s)).start()
 
         @pl.when(s == tp)
         def _():
-            pltpu.make_async_copy(AS.at[m, s], A.at[m, tp], arecv.at[m, tp]).start()
-
-    for c in loads[:4] + small[2:]:
+            pltpu.make_async_copy(AS.at[m, s], A.at[m, tp], arecv).start()
+
+    arrived(WIN, lsem.at[0])
+    for c in small[2:]:
         c.wait()
     own.wait()
-    arrived(W.at[:, k, y], wloc.at[0])
-    rcopy(W.at[:, k, y], W.at[:, k, y], wsend, wsown.at[0], sibling).start()
+    arrived(W.at[:, k, y], wloc)
+    rcopy(W.at[:, k, y], W.at[:, k, y], wsend, wsown, sibling).start()
     rowf = lax.broadcasted_iota(jnp.int32, (SEQ, 128), 0)
 
     def gathered(s):
@@ -299,13 +278,7 @@
     def project(t):
         s = seq_of(t)
 
-        def w(d):
-            return G.at[ring(y, d) * 2 + (1 - k), rows(s), :]
-
-        arrived(w(0), sib.at[t, 0])
-        arrived(w(-1), sib.at[t, 1])
-        arrived(w(1), sib.at[t, 2])
-        arrived(w(2), sib.at[t, 3])
+        arrived(G.at[pl.ds(0, 4), rows(s), :], sib.at[t])
         p = jnp.dot(gathered(s), WIN[...], preferred_element_type=F32)
         Q[rows(s), :] = p[:, 0:128].astype(BF16)
         mixed = p[:, 256:384] * p[:, 384:512]
@@ -315,10 +288,6 @@
         filt = tv[0:1] * m2 + tv[1:2] * m1 + tv[2:3] * mixed
         AS[0, s] = (p[:, 128:256] * filt).astype(BF16)
         send_branch(0, s)
-
-    def wkv(r, _):
-        arrived(KR.at[pl.ds(r * CAP, CAP)], kvr.at[r])
-        return 0
 
     def attend(ts):
         parts = [(seq_of(t), h) for t in ts for h in range(2)]
@@ -355,23 +324,18 @@
             arrived(g, agr.at[t, 0])
             h = G.at[gblk(-1), rows(s, 0, HALF), :]
             rcopy(h, h, gsend, agr.at[t, 2], dev_y(1)).start()
-            rcopy(g, g, gsend, sib.at[t, 1], sibling).start()
+            rcopy(g, g, gsend, sib.at[t], sibling).start()
             g2 = G.at[gblk(1), rows(s), :]
             arrived(g2, agr.at[t, 1])
             h2 = G.at[gblk(1), rows(s, HALF, HALF), :]
-            rcopy(h2, h2, gsend, agr.at[t, 3], dev_y(-1)).start()
-            rcopy(g2, g2, gsend, sib.at[t, 2], sibling).start()
+            rcopy(h2, h2, gsend, agr.at[t, 2], dev_y(-1)).start()
+            rcopy(g2, g2, gsend, sib.at[t], sibling).start()
 
         @pl.when(t < 6)
         def _():
             direct(t + 2)
 
-        @pl.when(t == 0)
-        def _():
-            plane1()
-            send_kv()
-
-        @pl.when(t == 2)
+        @pl.when(t == 3)
         def _():
             plane2()
 
@@ -379,23 +343,26 @@
         def _():
             u = t - 1
             s = seq_of(u)
-            arrived(G.at[gblk(2), rows(s, 0, HALF), :], agr.at[u, 2])
-            arrived(G.at[gblk(2), rows(s, HALF, HALF), :], agr.at[u, 3])
+            arrived(G.at[gblk(2), rows(s), :], agr.at[u, 2])
             g = G.at[gblk(2), rows(s), :]
-            rcopy(g, g, gsend, sib.at[u, 3], sibling).start()
+            rcopy(g, g, gsend, sib.at[u], sibling).start()
+
+        @pl.when(t == 8)
+        def _():
+            attend2(2, 0)
 
         @pl.when(t >= 2)
         def _():
             project(t - 2)
 
-        @pl.when(t == 6)
-        def _():
-            lax.fori_loop(0, NST, wkv, 0)
+        @pl.when(t == 7)
+        def _():
+            arrived(KR, kvr)
             pcopy.wait()
 
-        @pl.when((t == 6) | (t == 7))
-        def _():
-            lax.fori_loop((t - 6) * 2, t - 4, attend2, 0)
+        @pl.when(t == 7)
+        def _():
+            lax.fori_loop(0, 2, attend2, 0)
 
         @pl.when(t >= 8)
         def _():
@@ -404,6 +371,7 @@
         @pl.when(t == 8)
         def _():
             plane3()
+
 
         return 0
 
@@ -417,23 +385,11 @@
     mix0 = mix[:, 0:1]
     mix1 = mix[:, 1:2]
 
-    def wa(j, _):
-        arrived(A.at[0, j], arecv.at[0, j])
-        arrived(A.at[1, j], arecv.at[1, j])
-        return 0
-
-    lax.fori_loop(0, NTP, wa, 0)
-
-    def wws(j, _):
-        for d in range(4):
-            bs = lax.rem((1 - k) * x + k * z + d, 4)
-            i = lax.div(j, 3)
-            blk = (1 - k) * (i * NXZ + bs) + k * (bs * NXZ + i)
-            arrived(W.at[blk, 1 - k, yo(lax.rem(j, 3) + 1)], wsib.at[d, j])
-        return 0
-
-    arrived(W.at[:, 1 - k, y], wsown.at[0])
-    lax.fori_loop(0, 12, wws, 0)
+    arrived(A, arecv)
+
+    arrived(W.at[:, 1 - k, y], wsown)
+    for d in range(4):
+        arrived(TWELVE, wsib.at[d])
 
     order = [(kk, yy) for kk in range(2) for yy in range(4)]
 
@@ -449,11 +405,18 @@
                 axis=1,
             )
             acc.append(jnp.dot(lhs, rhs, preferred_element_type=F32))
-        out[:, pl.ds(pl.multiple_of(c * 256, 256), 256)] = (mix0 * acc[0] + mix1 * acc[1]).astype(BF16)
-        return 0
+        OB[c] = (mix0 * acc[0] + mix1 * acc[1]).astype(BF16)
+        put(c).start()
+        return 0
+
+    def put(c):
+        return pltpu.make_async_copy(
+            OB.at[c], out.at[:, pl.ds(pl.multiple_of(c * 256, 256), 256)], osem
+        )
 
     lax.fori_loop(0, 8, outp, 0)
 
+    arrived(OB, osem)
     arrived(OV.at[pl.ds(0, NST - 1)], ixs)
     arrived(KS.at[pl.ds(0, NST - 1)], kvs)
     arrived(G.at[pl.ds(0, 7)], gsend)
@@ -465,15 +428,15 @@
     tokens, store, holder, slot, wq, wk, wval, wo, wi, wv, taps, route, cout, mout
 ):
     hbm = pl.BlockSpec(memory_space=pltpu.HBM)
-    vmem = pl.BlockSpec(memory_space=pltpu.VMEM)
     dma = pltpu.SemaphoreType.DMA
     V = pltpu.VMEM
     return pl.pallas_call(
         kernel,
         out_shape=jax.ShapeDtypeStruct((SEQ, cout.shape[1]), BF16),
         in_specs=[hbm] * 14,
-        out_specs=vmem,
+        out_specs=pl.BlockSpec(memory_space=pl.ANY),
         scratch_shapes=[
+            V((8, SEQ, 256), BF16),
             pltpu.SMEM((2, 16), jnp.int32),
             pltpu.SMEM((2, 16), jnp.int32),
             V((3, 128), BF16),
@@ -494,9 +457,9 @@
             V((2, 8, SEQ, 128), BF16),
             V((2, 8, SEQ, 128), BF16),
             V((NST, 2, 4, 2, 128, 128), BF16),
-            dma((13,)), dma((8,)), dma((NST,)), dma, dma((NST,)), dma,
-            dma((8, 4)), dma((8, 4)), dma, dma((2, 8)), dma,
-            dma((1,)), dma((6,)), dma((9,)), dma((3, 12)), dma((4, 12)), dma((1,)), dma,
+            dma((8,)), dma((8,)), dma, dma, dma, dma,
+            dma((8, 3)), dma((8,)), dma, dma, dma,
+            dma, dma, dma, dma((3,)), dma((4,)), dma, dma, dma,
         ],
         compiler_params=pltpu.CompilerParams(
             collective_id=0, has_side_effects=True, vmem_limit_bytes=44 * 1024 * 1024

time: 79.2 us -> 68.7 us (0.87)
  Pallas kernels: 78.2 us -> 67.6 us
    pallas_call x1, Pallas kernels: 78.2 us -> 67.6 us  [local(): pl.pallas_call(kernel, out_shape=jax.ShapeDtypeStruct((SEQ, cout.shape[1]...]
where the time goes in v3:
time: 68.7 us; the launch traced here: 68.6 us
  Pallas kernels  67.6 us (98%)
  local copies, waits for them, and re-layouts  0.97 us (1%)
    pallas_call x1, Pallas kernels, local(): pl.pallas_call(kernel, out_shape=jax.ShapeDtypeStruct((SEQ, cout.shape[1]...  67.6 us

profile of v3, /device:TPU:25, one launch (start us, length us, event | category | flops | bytes accessed | tf_op | source)
XLA Modules:
  0.0 68.6 jit_solution(2580718251653336217)
XLA Ops:
  0.0 67.6 %shard_map.136 = bf16[256,2048]{1,0:T(8,128)(2,1)S(1)} custom-call(bf16[2048,256]{1,0:T(8,128)(2,1)} %tokens.1, bf16[2048,2048]{1,0:T(8,128)(2,1)} %bitcast.4, s32[2,16]{1,0:T(2,128)} %bitcast.6, s32[2,16]{1,0:T(2,128)} %bitcast.7, bf16[2048,128]{1,0:T(8,128)(2,1)} %wq.1, bf16[2048,128]{1,0:T(8,128)(2,1)} %wo.1, bf16[2048,128]{1,0:T(8,128)(2,1)} %wi.1, ...), custom_call_target="tpu_custom_call" | custom-call | tf_op jit(solution)/shard_map/pallas_call | solution.py:433
  67.6 1.0 %copy.16 = bf16[256,2048]{1,0:T(8,128)(2,1)} copy(bf16[256,2048]{1,0:T(8,128)(2,1)S(1)} %shard_map.136) | data formatting | bytes 2097152

commit v4 on v3

--- a/solution.py
+++ b/solution.py
@@ -14,6 +14,7 @@
 NXZ = 4
 NST = 16
 NTP = 8
+STEP = 32
 MESH = pl.DeviceIdType.MESH
 F32 = jnp.float32
 BF16 = jnp.bfloat16
@@ -22,7 +23,7 @@
 def kernel(
     tokens, store, holder_h, slot_h, wq, wo, wi, wv, wk, wval, taps_h, route_h, cout, mout,
     out,
-    OB, holder, slot, taps, route, G, ST, WIN, WKV, TB, KS, KR, OV, WV, WS, PV, PS, Q, AS, A, W,
+    AC, PM, OB, holder, slot, taps, route, G, ST, WIN, WKV, TB, KS, KR, OV, WV, WS, PV, PS, Q, AS, A, W,
     lsem, stsem, ixr, ixs, kvr, kvs, agr, sib, gsend, arecv, asend,
     wloc, w1, p1, p2, wsib, wsown, wsend, osem,
 ):
@@ -55,11 +56,8 @@
     def arrived(ref, sem):
         pltpu.make_async_copy(ref, ref, sem).wait()
 
-    def seq_of(t):
-        return lax.rem(t, 4) * 2 + lax.div(t, 4)
-
-    def rows(s, lo=0, n=SEQ):
-        return pl.ds(pl.multiple_of(s * SEQ + lo, 64), n)
+    def rows(t):
+        return pl.ds(pl.multiple_of(t * STEP, STEP), STEP)
 
     bar = pltpu.get_barrier_semaphore()
 
@@ -142,9 +140,8 @@
     pltpu.make_async_copy(OV.at[st], WV.at[st], ixr).start()
 
     def direct(t):
-        s = seq_of(t)
-        src = tokens.at[rows(s), :]
-        dst = G.at[tp, rows(s), :]
+        src = tokens.at[:, rows(t), :]
+        dst = G.at[tp, :, rows(t), :]
         rcopy(src, dst, gsend, agr.at[t, 0], dev_y(1)).start()
         rcopy(src, dst, gsend, agr.at[t, 1], dev_y(-1)).start()
         rcopy(src, dst, gsend, sib.at[t], sibling).start()
@@ -175,7 +172,7 @@
             TB[i * 4 + j] = kv[j * PLEN : (j + 1) * PLEN]
         return 0
 
-    lax.fori_loop(0, 8, kv_body, 0)
+    lax.fori_loop(0, 6, kv_body, 0)
 
     def send_kv():
         arrived(WV, ixr)
@@ -218,13 +215,13 @@
     def wblk(j, d):
         return W.at[stidx(lax.div(j, 3), ring(b, d)), k, yo(lax.rem(j, 3) + 1)]
 
-    def wpass(d, sem, dev):
+    def wpass(lo, hi, d, sem, dev):
         def go(j, _):
             g = wblk(j, d)
             rcopy(g, g, wsend, sem, dev).start()
             return 0
 
-        lax.fori_loop(0, 12, go, 0)
+        lax.fori_loop(lo, hi, go, 0)
 
     TWELVE = W.at[pl.ds(0, 3), 0]
 
@@ -238,30 +235,34 @@
             return 0
 
         lax.fori_loop(0, 12, go, 0)
-        wpass(0, p2.at[2], dev_b(2))
-        wpass(0, wsib.at[0], sibling)
+        wpass(0, 12, 0, wsib.at[0], sibling)
 
     def plane3():
         arrived(TWELVE, p2.at[0])
-        wpass(-1, wsib.at[1], sibling)
         arrived(TWELVE, p2.at[1])
-        wpass(1, wsib.at[2], sibling)
+        wpass(0, 6, -1, p2.at[2], dev_b(1))
+        wpass(6, 12, 1, p2.at[2], dev_b(-1))
+        wpass(0, 12, -1, wsib.at[1], sibling)
+        wpass(0, 12, 1, wsib.at[2], sibling)
 
     def plane4():
         arrived(TWELVE, p2.at[2])
-        wpass(2, wsib.at[3], sibling)
+        wpass(0, 12, 2, wsib.at[3], sibling)
 
     plane1()
+    lax.fori_loop(6, 8, kv_body, 0)
     send_kv()
 
-    def send_branch(m, s):
-        @pl.when(s != tp)
-        def _():
-            rcopy(AS.at[m, s], A.at[m, tp], asend, arecv, (st, s)).start()
-
-        @pl.when(s == tp)
-        def _():
-            pltpu.make_async_copy(AS.at[m, s], A.at[m, tp], arecv).start()
+    def send_branch(m, lo, n):
+        r = pl.ds(pl.multiple_of(lo, STEP), n)
+
+        def go(d, _):
+            s = lax.rem(tp + d, NTP)
+            rcopy(AS.at[m, s, r, :], A.at[m, tp, r, :], asend, arecv.at[m], (st, s)).start()
+            return 0
+
+        lax.fori_loop(1, NTP, go, 0)
+        pltpu.make_async_copy(AS.at[m, tp, r, :], A.at[m, tp, r, :], arecv.at[m]).start()
 
     arrived(WIN, lsem.at[0])
     for c in small[2:]:
@@ -269,65 +270,57 @@
     own.wait()
     arrived(W.at[:, k, y], wloc)
     rcopy(W.at[:, k, y], W.at[:, k, y], wsend, wsown, sibling).start()
-    rowf = lax.broadcasted_iota(jnp.int32, (SEQ, 128), 0)
-
-    def gathered(s):
-        r = rows(s)
-        return jnp.concatenate([G[j, r, :] for j in range(NTP)], axis=1)
+    PM[...] = jnp.zeros_like(PM)
+    place = lax.rem(lax.broadcasted_iota(jnp.int32, (SEQ, 128), 0), STEP)
 
     def project(t):
-        s = seq_of(t)
-
-        arrived(G.at[pl.ds(0, 4), rows(s), :], sib.at[t])
-        p = jnp.dot(gathered(s), WIN[...], preferred_element_type=F32)
-        Q[rows(s), :] = p[:, 0:128].astype(BF16)
+        arrived(G.at[pl.ds(0, 4), :, rows(t), :], sib.at[t])
+        rws = jnp.concatenate([G[j, :, rows(t), :].reshape(SEQ, 256) for j in range(NTP)], axis=1)
+        p = jnp.dot(rws, WIN[...], preferred_element_type=F32)
+        Q[:, rows(t), :] = p[:, 0:128].astype(BF16).reshape(NTP, STEP, 128)
         mixed = p[:, 256:384] * p[:, 384:512]
+        prev = PM[...]
+        PM[...] = mixed
         tv = taps[...].astype(F32)
-        m1 = jnp.where(rowf >= 1, pltpu.roll(mixed, 1, 0), 0.0)
-        m2 = jnp.where(rowf >= 2, pltpu.roll(mixed, 2, 0), 0.0)
+        m1 = jnp.where(place >= 1, pltpu.roll(mixed, 1, 0), pltpu.roll(prev, SEQ + 1 - STEP, 0))
+        m2 = jnp.where(place >= 2, pltpu.roll(mixed, 2, 0), pltpu.roll(prev, SEQ + 2 - STEP, 0))
         filt = tv[0:1] * m2 + tv[1:2] * m1 + tv[2:3] * mixed
-        AS[0, s] = (p[:, 128:256] * filt).astype(BF16)
-        send_branch(0, s)
-
-    def attend(ts):
-        parts = [(seq_of(t), h) for t in ts for h in range(2)]
+        AS[0, :, rows(t), :] = (p[:, 128:256] * filt).astype(BF16).reshape(NTP, STEP, 128)
+        send_branch(0, t * STEP, STEP)
+
+    def attend(seqs, lo, n):
         kvs_, sc = [], []
-        for s, h in parts:
-            n = (s * 2 + h) * 2
-            kv = jnp.concatenate([KR[PS[n, 0, 0]], KR[PS[n + 1, 0, 0]]], axis=0)
-            q = Q[rows(s, h * BLOCK, BLOCK), :]
+        for s in seqs:
+            i = (s * 2 + lo // BLOCK) * 2
+            kv = jnp.concatenate([KR[PS[i, 0, 0]], KR[PS[i + 1, 0, 0]]], axis=0)
             kvs_.append(kv)
             sc.append(
                 lax.dot_general(
-                    q, kv[:, :128], (((1,), (1,)), ((), ())), preferred_element_type=F32
+                    Q[s, lo : lo + n, :], kv[:, :128], (((1,), (1,)), ((), ())), preferred_element_type=F32
                 ) * (HEAD_SIZE ** -0.5)
             )
         e = [jnp.exp(v - jnp.max(v, axis=1, keepdims=True)) for v in sc]
         wt = [(v / jnp.sum(v, axis=1, keepdims=True)).astype(BF16) for v in e]
-        for (s, h), kv, v in zip(parts, kvs_, wt):
+        for s, kv, v in zip(seqs, kvs_, wt):
             o = jnp.dot(v, kv[:, 128:], preferred_element_type=F32)
-            AS[1, s, pl.ds(h * BLOCK, BLOCK), :] = o.astype(BF16)
-        for t in ts:
-            send_branch(1, seq_of(t))
-
-    def attend2(i, _):
-        attend([2 * i, 2 * i + 1])
-        return 0
-
-    HALF = SEQ // 2
+            AS[1, s, lo : lo + n, :] = o.astype(BF16)
+
+    def attend4(i, _):
+        attend([i * 4 + j for j in range(4)], 0, BLOCK)
+        return 0
 
     def step(t, _):
         @pl.when(t < 8)
         def _():
-            s = seq_of(t)
-            g = G.at[gblk(-1), rows(s), :]
+            r = rows(t)
+            g = G.at[gblk(-1), :, r, :]
             arrived(g, agr.at[t, 0])
-            h = G.at[gblk(-1), rows(s, 0, HALF), :]
+            h = G.at[gblk(-1), pl.ds(0, 4), r, :]
             rcopy(h, h, gsend, agr.at[t, 2], dev_y(1)).start()
             rcopy(g, g, gsend, sib.at[t], sibling).start()
-            g2 = G.at[gblk(1), rows(s), :]
+            g2 = G.at[gblk(1), :, r, :]
             arrived(g2, agr.at[t, 1])
-            h2 = G.at[gblk(1), rows(s, HALF, HALF), :]
+            h2 = G.at[gblk(1), pl.ds(4, 4), r, :]
             rcopy(h2, h2, gsend, agr.at[t, 2], dev_y(-1)).start()
             rcopy(g2, g2, gsend, sib.at[t], sibling).start()
 
@@ -342,14 +335,14 @@
         @pl.when((t >= 1) & (t < 9))
         def _():
             u = t - 1
-            s = seq_of(u)
-            arrived(G.at[gblk(2), rows(s), :], agr.at[u, 2])
-            g = G.at[gblk(2), rows(s), :]
+            g = G.at[gblk(2), :, rows(u), :]
+            arrived(g, agr.at[u, 2])
             rcopy(g, g, gsend, sib.at[u], sibling).start()
 
         @pl.when(t == 8)
         def _():
-            attend2(2, 0)
+            attend(range(NTP), BLOCK, 64)
+            send_branch(1, BLOCK, 64)
 
         @pl.when(t >= 2)
         def _():
@@ -359,53 +352,46 @@
         def _():
             arrived(KR, kvr)
             pcopy.wait()
-
-        @pl.when(t == 7)
-        def _():
-            lax.fori_loop(0, 2, attend2, 0)
-
-        @pl.when(t >= 8)
-        def _():
-            attend([t - 2])
-
-        @pl.when(t == 8)
-        def _():
+            lax.fori_loop(0, 2, attend4, 0)
+            send_branch(1, 0, BLOCK)
             plane3()
 
-
         return 0
 
     lax.fori_loop(0, 10, step, 0)
+    attend(range(NTP), BLOCK + 64, 64)
+    send_branch(1, BLOCK + 64, 64)
     plane4()
-
-    logits = lax.dot_general(
-        gathered(tp), route[...], (((1,), (1,)), ((), ())), preferred_element_type=F32
-    )
+    rws = jnp.concatenate([G[j, tp] for j in range(NTP)], axis=1)
+    logits = lax.dot_general(rws, route[...], (((1,), (1,)), ((), ())), preferred_element_type=F32)
     mix = jax.nn.sigmoid(logits)
     mix0 = mix[:, 0:1]
     mix1 = mix[:, 1:2]
 
-    arrived(A, arecv)
-
+    arrived(A.at[0], arecv.at[0])
     arrived(W.at[:, 1 - k, y], wsown)
     for d in range(4):
         arrived(TWELVE, wsib.at[d])
 
     order = [(kk, yy) for kk in range(2) for yy in range(4)]
 
+    def branch(c, m):
+        lhs = jnp.concatenate([A[m, yy * 2 + kk] for kk, yy in order], axis=1)
+        rhs = jnp.concatenate(
+            [
+                jnp.concatenate([W[c * 2 + h, kk, yy, m] for kk, yy in order], axis=0)
+                for h in range(2)
+            ],
+            axis=1,
+        )
+        return jnp.dot(lhs, rhs, preferred_element_type=F32)
+
+    def outc(c, _):
+        AC[c] = mix0 * branch(c, 0)
+        return 0
+
     def outp(c, _):
-        acc = []
-        for m in range(2):
-            lhs = jnp.concatenate([A[m, yy * 2 + kk] for kk, yy in order], axis=1)
-            rhs = jnp.concatenate(
-                [
-                    jnp.concatenate([W[c * 2 + h, kk, yy, m] for kk, yy in order], axis=0)
-                    for h in range(2)
-                ],
-                axis=1,
-            )
-            acc.append(jnp.dot(lhs, rhs, preferred_element_type=F32))
-        OB[c] = (mix0 * acc[0] + mix1 * acc[1]).astype(BF16)
+        OB[c] = (AC[c] + mix1 * branch(c, 1)).astype(BF16)
         put(c).start()
         return 0
 
@@ -414,6 +400,8 @@
             OB.at[c], out.at[:, pl.ds(pl.multiple_of(c * 256, 256), 256)], osem
         )
 
+    lax.fori_loop(0, 8, outc, 0)
+    arrived(A.at[1], arecv.at[1])
     lax.fori_loop(0, 8, outp, 0)
 
     arrived(OB, osem)
@@ -436,12 +424,14 @@
         in_specs=[hbm] * 14,
         out_specs=pl.BlockSpec(memory_space=pl.ANY),
         scratch_shapes=[
+            V((8, SEQ, 256), F32),
+            V((SEQ, 128), F32),
             V((8, SEQ, 256), BF16),
             pltpu.SMEM((2, 16), jnp.int32),
             pltpu.SMEM((2, 16), jnp.int32),
             V((3, 128), BF16),
             V((2, 2048), BF16),
-            V((8, 2048, 256), BF16),
+            V((8, NTP, SEQ, 256), BF16),
             V((2048, 2048), BF16),
             V((2048, 512), BF16),
             V((2048, 256), BF16),
@@ -453,12 +443,12 @@
             pltpu.SMEM((NST, 1, 128), jnp.int32),
             V((32, 1, 128), jnp.int32),
             pltpu.SMEM((32, 1, 128), jnp.int32),
-            V((2048, 128), BF16),
+            V((NTP, SEQ, 128), BF16),
             V((2, 8, SEQ, 128), BF16),
             V((2, 8, SEQ, 128), BF16),
             V((NST, 2, 4, 2, 128, 128), BF16),
             dma((8,)), dma((8,)), dma, dma, dma, dma,
-            dma((8, 3)), dma((8,)), dma, dma, dma,
+            dma((8, 3)), dma((8,)), dma, dma((2,)), dma,
             dma, dma, dma, dma((3,)), dma((4,)), dma, dma, dma,
         ],
         compiler_params=pltpu.CompilerParams(
@@ -468,7 +458,7 @@
         *(
             pltpu.with_memory_space_constraint(v, pltpu.HBM)
             for v in (
-                tokens, store.reshape(-1, store.shape[-1]), holder.T, slot.T,
+                tokens.reshape(NTP, SEQ, tokens.shape[1]), store.reshape(-1, store.shape[-1]), holder.T, slot.T,
                 wq, wo, wi, wv, wk, wval, taps, route.T, cout, mout,
             )
         )

time: 68.7 us -> 68.6 us (level)
  the two profiles are of different devices: /device:TPU:25 before, /device:TPU:1 now
where the time goes in v4:
time: 68.6 us; the launch traced here: 67.9 us
  Pallas kernels  67 us (98%)
  local copies, waits for them, and re-layouts  0.97 us (1%)
    pallas_call x1, Pallas kernels, local(): pl.pallas_call(kernel, out_shape=jax.ShapeDtypeStruct((SEQ, cout.shape[1]...  67 us

profile of v4, /device:TPU:1, one launch (start us, length us, event | category | flops | bytes accessed | tf_op | source)
XLA Modules:
  0.0 67.9 jit_solution(9707442435409268282)
XLA Ops:
  0.0 67.0 %shard_map.136 = bf16[256,2048]{1,0:T(8,128)(2,1)S(1)} custom-call(bf16[8,256,256]{2,1,0:T(8,128)(2,1)} %bitcast.6, bf16[2048,2048]{1,0:T(8,128)(2,1)} %bitcast.5, s32[2,16]{1,0:T(2,128)} %bitcast.8, s32[2,16]{1,0:T(2,128)} %bitcast.9, bf16[2048,128]{1,0:T(8,128)(2,1)} %wq.1, bf16[2048,128]{1,0:T(8,128)(2,1)} %wo.1, bf16[2048,128]{1,0:T(8,128)(2,1)} %wi.1, ...), custom_call_target="tpu_custom_call" | custom-call | tf_op jit(solution)/shard_map/pallas_call | solution.py:421
  67.0 1.0 %copy.16 = bf16[256,2048]{1,0:T(8,128)(2,1)} copy(bf16[256,2048]{1,0:T(8,128)(2,1)S(1)} %shard_map.136) | data formatting | bytes 2097152

commit v5 on v4

--- a/solution.py
+++ b/solution.py
@@ -15,6 +15,8 @@
 NST = 16
 NTP = 8
 STEP = 32
+WIDE = 512
+RELAYED = 8
 MESH = pl.DeviceIdType.MESH
 F32 = jnp.float32
 BF16 = jnp.bfloat16
@@ -23,7 +25,7 @@
 def kernel(
     tokens, store, holder_h, slot_h, wq, wo, wi, wv, wk, wval, taps_h, route_h, cout, mout,
     out,
-    AC, PM, OB, holder, slot, taps, route, G, ST, WIN, WKV, TB, KS, KR, OV, WV, WS, PV, PS, Q, AS, A, W,
+    PM, OB, holder, slot, taps, route, G, ST, WIN, WKV, TB, KS, KR, OV, WV, WS, PV, PS, Q, AS, A, W,
     lsem, stsem, ixr, ixs, kvr, kvs, agr, sib, gsend, arecv, asend,
     wloc, w1, p1, p2, wsib, wsown, wsend, osem,
 ):
@@ -146,6 +148,10 @@
         rcopy(src, dst, gsend, agr.at[t, 1], dev_y(-1)).start()
         rcopy(src, dst, gsend, sib.at[t], sibling).start()
 
+        @pl.when(t >= RELAYED)
+        def _():
+            rcopy(src, dst, gsend, agr.at[t, 2], dev_y(2)).start()
+
     def gblk(d):
         return ring(y, d) * 2 + k
 
@@ -223,29 +229,27 @@
 
         lax.fori_loop(lo, hi, go, 0)
 
+    SIX = W.at[pl.ds(0, 6), 0, 0]
     TWELVE = W.at[pl.ds(0, 3), 0]
 
     def plane2():
         arrived(W.at[pl.ds(0, 9), 0, 0], p1)
-
-        def go(j, _):
-            g = wblk(j, 0)
-            rcopy(g, g, wsend, p2.at[0], dev_b(1)).start()
-            rcopy(g, g, wsend, p2.at[1], dev_b(-1)).start()
-            return 0
-
-        lax.fori_loop(0, 12, go, 0)
+        wpass(0, 6, 0, p2.at[0], dev_b(1))
+        wpass(6, 12, 0, p2.at[1], dev_b(-1))
         wpass(0, 12, 0, wsib.at[0], sibling)
 
     def plane3():
-        arrived(TWELVE, p2.at[0])
-        arrived(TWELVE, p2.at[1])
+        arrived(SIX, p2.at[0])
+        arrived(SIX, p2.at[1])
         wpass(0, 6, -1, p2.at[2], dev_b(1))
         wpass(6, 12, 1, p2.at[2], dev_b(-1))
-        wpass(0, 12, -1, wsib.at[1], sibling)
-        wpass(0, 12, 1, wsib.at[2], sibling)
+        wpass(0, 6, -1, wsib.at[1], sibling)
+        wpass(6, 12, 1, wsib.at[1], sibling)
 
     def plane4():
+        arrived(TWELVE, p2.at[3])
+        wpass(6, 12, -1, wsib.at[2], sibling)
+        wpass(0, 6, 1, wsib.at[2], sibling)
         arrived(TWELVE, p2.at[2])
         wpass(0, 12, 2, wsib.at[3], sibling)
 
@@ -258,11 +262,11 @@
 
         def go(d, _):
             s = lax.rem(tp + d, NTP)
-            rcopy(AS.at[m, s, r, :], A.at[m, tp, r, :], asend, arecv.at[m], (st, s)).start()
+            rcopy(AS.at[m, s, r, :], A.at[m, tp, r, :], asend, arecv, (st, s)).start()
             return 0
 
         lax.fori_loop(1, NTP, go, 0)
-        pltpu.make_async_copy(AS.at[m, tp, r, :], A.at[m, tp, r, :], arecv.at[m]).start()
+        pltpu.make_async_copy(AS.at[m, tp, r, :], A.at[m, tp, r, :], arecv).start()
 
     arrived(WIN, lsem.at[0])
     for c in small[2:]:
@@ -305,9 +309,18 @@
             o = jnp.dot(v, kv[:, 128:], preferred_element_type=F32)
             AS[1, s, lo : lo + n, :] = o.astype(BF16)
 
-    def attend4(i, _):
-        attend([i * 4 + j for j in range(4)], 0, BLOCK)
-        return 0
+    def send_memory(i):
+        r = pl.ds(0, BLOCK)
+        for j in range(4):
+            s = i * 4 + j
+
+            @pl.when(s != tp)
+            def _():
+                rcopy(AS.at[1, s, r, :], A.at[1, tp, r, :], asend, arecv, (st, s)).start()
+
+            @pl.when(s == tp)
+            def _():
+                pltpu.make_async_copy(AS.at[1, s, r, :], A.at[1, tp, r, :], arecv).start()
 
     def step(t, _):
         @pl.when(t < 8)
@@ -316,12 +329,20 @@
             g = G.at[gblk(-1), :, r, :]
             arrived(g, agr.at[t, 0])
             h = G.at[gblk(-1), pl.ds(0, 4), r, :]
-            rcopy(h, h, gsend, agr.at[t, 2], dev_y(1)).start()
+
+            @pl.when(t < RELAYED)
+            def _():
+                rcopy(h, h, gsend, agr.at[t, 2], dev_y(1)).start()
+
             rcopy(g, g, gsend, sib.at[t], sibling).start()
             g2 = G.at[gblk(1), :, r, :]
             arrived(g2, agr.at[t, 1])
             h2 = G.at[gblk(1), pl.ds(4, 4), r, :]
-            rcopy(h2, h2, gsend, agr.at[t, 2], dev_y(-1)).start()
+
+            @pl.when(t < RELAYED)
+            def _():
+                rcopy(h2, h2, gsend, agr.at[t, 2], dev_y(-1)).start()
+
             rcopy(g2, g2, gsend, sib.at[t], sibling).start()
 
         @pl.when(t < 6)
@@ -332,13 +353,24 @@
         def _():
             plane2()
 
-        @pl.when((t >= 1) & (t < 9))
-        def _():
-            u = t - 1
+        @pl.when(t == 5)
+        def _():
+            wpass(6, 12, 0, p2.at[3], dev_b(1))
+            wpass(0, 6, 0, p2.at[3], dev_b(-1))
+
+        @pl.when(t == 6)
+        def _():
+            plane3()
+
+        def opposite(u):
             g = G.at[gblk(2), :, rows(u), :]
             arrived(g, agr.at[u, 2])
             rcopy(g, g, gsend, sib.at[u], sibling).start()
 
+        @pl.when((t >= 1) & (t < 9))
+        def _():
+            opposite(t - 1)
+
         @pl.when(t == 8)
         def _():
             attend(range(NTP), BLOCK, 64)
@@ -348,13 +380,15 @@
         def _():
             project(t - 2)
 
-        @pl.when(t == 7)
+        @pl.when(t == 6)
         def _():
             arrived(KR, kvr)
             pcopy.wait()
-            lax.fori_loop(0, 2, attend4, 0)
-            send_branch(1, 0, BLOCK)
-            plane3()
+
+        @pl.when((t == 6) | (t == 7))
+        def _():
+            attend([(t - 6) * 4 + j for j in range(4)], 0, BLOCK)
+            send_memory(t - 6)
 
         return 0
 
@@ -365,44 +399,36 @@
     rws = jnp.concatenate([G[j, tp] for j in range(NTP)], axis=1)
     logits = lax.dot_general(rws, route[...], (((1,), (1,)), ((), ())), preferred_element_type=F32)
     mix = jax.nn.sigmoid(logits)
-    mix0 = mix[:, 0:1]
-    mix1 = mix[:, 1:2]
-
-    arrived(A.at[0], arecv.at[0])
+
     arrived(W.at[:, 1 - k, y], wsown)
     for d in range(4):
         arrived(TWELVE, wsib.at[d])
 
     order = [(kk, yy) for kk in range(2) for yy in range(4)]
 
-    def branch(c, m):
-        lhs = jnp.concatenate([A[m, yy * 2 + kk] for kk, yy in order], axis=1)
-        rhs = jnp.concatenate(
-            [
-                jnp.concatenate([W[c * 2 + h, kk, yy, m] for kk, yy in order], axis=0)
-                for h in range(2)
-            ],
-            axis=1,
-        )
-        return jnp.dot(lhs, rhs, preferred_element_type=F32)
-
-    def outc(c, _):
-        AC[c] = mix0 * branch(c, 0)
-        return 0
-
-    def outp(c, _):
-        OB[c] = (AC[c] + mix1 * branch(c, 1)).astype(BF16)
-        put(c).start()
-        return 0
-
     def put(c):
         return pltpu.make_async_copy(
-            OB.at[c], out.at[:, pl.ds(pl.multiple_of(c * 256, 256), 256)], osem
+            OB.at[c], out.at[:, pl.ds(pl.multiple_of(c * WIDE, WIDE), WIDE)], osem
         )
 
-    lax.fori_loop(0, 8, outc, 0)
-    arrived(A.at[1], arecv.at[1])
-    lax.fori_loop(0, 8, outp, 0)
+    def outp(c, _):
+        acc = []
+        for m in range(2):
+            lhs = jnp.concatenate([A[m, yy * 2 + kk] for kk, yy in order], axis=1)
+            rhs = jnp.concatenate(
+                [
+                    jnp.concatenate([W[c * (WIDE // 128) + i, kk, yy, m] for kk, yy in order], axis=0)
+                    for i in range(WIDE // 128)
+                ],
+                axis=1,
+            )
+            acc.append(jnp.dot(lhs, rhs, preferred_element_type=F32))
+        OB[c] = (mix[:, 0:1] * acc[0] + mix[:, 1:2] * acc[1]).astype(BF16)
+        put(c).start()
+        return 0
+
+    arrived(A, arecv)
+    lax.fori_loop(0, 2048 // WIDE, outp, 0)
 
     arrived(OB, osem)
     arrived(OV.at[pl.ds(0, NST - 1)], ixs)
@@ -424,9 +450,8 @@
         in_specs=[hbm] * 14,
         out_specs=pl.BlockSpec(memory_space=pl.ANY),
         scratch_shapes=[
-            V((8, SEQ, 256), F32),
             V((SEQ, 128), F32),
-            V((8, SEQ, 256), BF16),
+            V((2048 // WIDE, SEQ, WIDE), BF16),
             pltpu.SMEM((2, 16), jnp.int32),
             pltpu.SMEM((2, 16), jnp.int32),
             V((3, 128), BF16),
@@ -448,8 +473,8 @@
             V((2, 8, SEQ, 128), BF16),
             V((NST, 2, 4, 2, 128, 128), BF16),
             dma((8,)), dma((8,)), dma, dma, dma, dma,
-            dma((8, 3)), dma((8,)), dma, dma((2,)), dma,
-            dma, dma, dma, dma((3,)), dma((4,)), dma, dma, dma,
+            dma((8, 3)), dma((8,)), dma, dma, dma,
+            dma, dma, dma, dma((4,)), dma((4,)), dma, dma, dma,
         ],
         compiler_params=pltpu.CompilerParams(
             collective_id=0, has_side_effects=True, vmem_limit_bytes=44 * 1024 * 1024

time: 68.6 us -> 66.5 us (0.969)
  Pallas kernels: 67 us -> 65.4 us
    pallas_call x1, Pallas kernels: 67 us -> 65.4 us  [local(): pl.pallas_call(kernel, out_shape=jax.ShapeDtypeStruct((SEQ, cout.shape[1]...]
where the time goes in v5:
time: 66.5 us; the launch traced here: 66.4 us
  Pallas kernels  65.4 us (98%)
  local copies, waits for them, and re-layouts  0.97 us (1%)
    pallas_call x1, Pallas kernels, local(): pl.pallas_call(kernel, out_shape=jax.ShapeDtypeStruct((SEQ, cout.shape[1]...  65.4 us

profile of v5, /device:TPU:1, one launch (start us, length us, event | category | flops | bytes accessed | tf_op | source)
XLA Modules:
  0.0 66.4 jit_solution(15904069067201914112)
XLA Ops:
  0.0 65.4 %shard_map.136 = bf16[256,2048]{1,0:T(8,128)(2,1)S(1)} custom-call(bf16[8,256,256]{2,1,0:T(8,128)(2,1)} %bitcast.6, bf16[2048,2048]{1,0:T(8,128)(2,1)} %bitcast.5, s32[2,16]{1,0:T(2,128)} %bitcast.8, s32[2,16]{1,0:T(2,128)} %bitcast.9, bf16[2048,128]{1,0:T(8,128)(2,1)} %wq.1, bf16[2048,128]{1,0:T(8,128)(2,1)} %wo.1, bf16[2048,128]{1,0:T(8,128)(2,1)} %wi.1, ...), custom_call_target="tpu_custom_call" | custom-call | tf_op jit(solution)/shard_map/pallas_call | solution.py:447
  65.4 1.0 %copy.16 = bf16[256,2048]{1,0:T(8,128)(2,1)} copy(bf16[256,2048]{1,0:T(8,128)(2,1)S(1)} %shard_map.136) | data formatting | bytes 2097152

commit v6 on v5

--- a/solution.py
+++ b/solution.py
@@ -15,8 +15,7 @@
 NST = 16
 NTP = 8
 STEP = 32
-WIDE = 512
-RELAYED = 8
+WIDE = 1024
 MESH = pl.DeviceIdType.MESH
 F32 = jnp.float32
 BF16 = jnp.bfloat16
@@ -89,7 +88,7 @@
 
     def store_copy(i):
         r = pl.ds(pl.multiple_of(i * SEQ, SEQ), SEQ)
-        return pltpu.make_async_copy(store.at[r, :], ST.at[r, :], stsem.at[i])
+        return pltpu.make_async_copy(store.at[r, :], ST.at[r, :], stsem)
 
     def start_store(i, _):
         store_copy(i).start()
@@ -148,10 +147,6 @@
         rcopy(src, dst, gsend, agr.at[t, 1], dev_y(-1)).start()
         rcopy(src, dst, gsend, sib.at[t], sibling).start()
 
-        @pl.when(t >= RELAYED)
-        def _():
-            rcopy(src, dst, gsend, agr.at[t, 2], dev_y(2)).start()
-
     def gblk(d):
         return ring(y, d) * 2 + k
 
@@ -169,9 +164,9 @@
     direct(1)
 
     arrived(WKV, lsem.at[1])
+    arrived(ST, stsem)
 
     def kv_body(i, _):
-        store_copy(i).wait()
         r = pl.ds(pl.multiple_of(i * SEQ, SEQ), SEQ)
         kv = jnp.dot(ST[r, :], WKV[...], preferred_element_type=F32).astype(BF16)
         for j in range(4):
@@ -250,6 +245,8 @@
         arrived(TWELVE, p2.at[3])
         wpass(6, 12, -1, wsib.at[2], sibling)
         wpass(0, 6, 1, wsib.at[2], sibling)
+
+    def plane5():
         arrived(TWELVE, p2.at[2])
         wpass(0, 12, 2, wsib.at[3], sibling)
 
@@ -293,34 +290,23 @@
         send_branch(0, t * STEP, STEP)
 
     def attend(seqs, lo, n):
+        blk = lo // BLOCK if isinstance(lo, int) else 0
+        r = pl.ds(lo, n)
         kvs_, sc = [], []
         for s in seqs:
-            i = (s * 2 + lo // BLOCK) * 2
+            i = (s * 2 + blk) * 2
             kv = jnp.concatenate([KR[PS[i, 0, 0]], KR[PS[i + 1, 0, 0]]], axis=0)
             kvs_.append(kv)
             sc.append(
                 lax.dot_general(
-                    Q[s, lo : lo + n, :], kv[:, :128], (((1,), (1,)), ((), ())), preferred_element_type=F32
+                    Q[s, r, :], kv[:, :128], (((1,), (1,)), ((), ())), preferred_element_type=F32
                 ) * (HEAD_SIZE ** -0.5)
             )
         e = [jnp.exp(v - jnp.max(v, axis=1, keepdims=True)) for v in sc]
         wt = [(v / jnp.sum(v, axis=1, keepdims=True)).astype(BF16) for v in e]
         for s, kv, v in zip(seqs, kvs_, wt):
             o = jnp.dot(v, kv[:, 128:], preferred_element_type=F32)
-            AS[1, s, lo : lo + n, :] = o.astype(BF16)
-
-    def send_memory(i):
-        r = pl.ds(0, BLOCK)
-        for j in range(4):
-            s = i * 4 + j
-
-            @pl.when(s != tp)
-            def _():
-                rcopy(AS.at[1, s, r, :], A.at[1, tp, r, :], asend, arecv, (st, s)).start()
-
-            @pl.when(s == tp)
-            def _():
-                pltpu.make_async_copy(AS.at[1, s, r, :], A.at[1, tp, r, :], arecv).start()
+            AS[1, s, r, :] = o.astype(BF16)
 
     def step(t, _):
         @pl.when(t < 8)
@@ -329,20 +315,12 @@
             g = G.at[gblk(-1), :, r, :]
             arrived(g, agr.at[t, 0])
             h = G.at[gblk(-1), pl.ds(0, 4), r, :]
-
-            @pl.when(t < RELAYED)
-            def _():
-                rcopy(h, h, gsend, agr.at[t, 2], dev_y(1)).start()
-
+            rcopy(h, h, gsend, agr.at[t, 2], dev_y(1)).start()
             rcopy(g, g, gsend, sib.at[t], sibling).start()
             g2 = G.at[gblk(1), :, r, :]
             arrived(g2, agr.at[t, 1])
             h2 = G.at[gblk(1), pl.ds(4, 4), r, :]
-
-            @pl.when(t < RELAYED)
-            def _():
-                rcopy(h2, h2, gsend, agr.at[t, 2], dev_y(-1)).start()
-
+            rcopy(h2, h2, gsend, agr.at[t, 2], dev_y(-1)).start()
             rcopy(g2, g2, gsend, sib.at[t], sibling).start()
 
         @pl.when(t < 6)
@@ -358,7 +336,7 @@
             wpass(6, 12, 0, p2.at[3], dev_b(1))
             wpass(0, 6, 0, p2.at[3], dev_b(-1))
 
-        @pl.when(t == 6)
+        @pl.when(t == 7)
         def _():
             plane3()
 
@@ -387,15 +365,19 @@
 
         @pl.when((t == 6) | (t == 7))
         def _():
-            attend([(t - 6) * 4 + j for j in range(4)], 0, BLOCK)
-            send_memory(t - 6)
+            attend(range(NTP), pl.multiple_of((t - 6) * 64, 64), 64)
+            send_branch(1, (t - 6) * 64, 64)
+
+        @pl.when(t == 8)
+        def _():
+            plane4()
 
         return 0
 
     lax.fori_loop(0, 10, step, 0)
     attend(range(NTP), BLOCK + 64, 64)
     send_branch(1, BLOCK + 64, 64)
-    plane4()
+    plane5()
     rws = jnp.concatenate([G[j, tp] for j in range(NTP)], axis=1)
     logits = lax.dot_general(rws, route[...], (((1,), (1,)), ((), ())), preferred_element_type=F32)
     mix = jax.nn.sigmoid(logits)
@@ -472,7 +454,7 @@
             V((2, 8, SEQ, 128), BF16),
             V((2, 8, SEQ, 128), BF16),
             V((NST, 2, 4, 2, 128, 128), BF16),
-            dma((8,)), dma((8,)), dma, dma, dma, dma,
+            dma((8,)), dma, dma, dma, dma, dma,
             dma((8, 3)), dma((8,)), dma, dma, dma,
             dma, dma, dma, dma((4,)), dma((4,)), dma, dma, dma,
         ],

time: 66.5 us -> 65.9 us (level)
  no operation moved by 1% of the time
where the time goes in v6:
time: 65.9 us; the launch traced here: 65.8 us
  Pallas kernels  64.8 us (98%)
  local copies, waits for them, and re-layouts  0.97 us (1%)
    pallas_call x1, Pallas kernels, local(): pl.pallas_call(kernel, out_shape=jax.ShapeDtypeStruct((SEQ, cout.shape[1]...  64.8 us

profile of v6, /device:TPU:1, one launch (start us, length us, event | category | flops | bytes accessed | tf_op | source)
XLA Modules:
  0.0 65.8 jit_solution(1532570411426816499)
XLA Ops:
  0.0 64.8 %shard_map.136 = bf16[256,2048]{1,0:T(8,128)(2,1)S(1)} custom-call(bf16[8,256,256]{2,1,0:T(8,128)(2,1)} %bitcast.6, bf16[2048,2048]{1,0:T(8,128)(2,1)} %bitcast.5, s32[2,16]{1,0:T(2,128)} %bitcast.8, s32[2,16]{1,0:T(2,128)} %bitcast.9, bf16[2048,128]{1,0:T(8,128)(2,1)} %wq.1, bf16[2048,128]{1,0:T(8,128)(2,1)} %wo.1, bf16[2048,128]{1,0:T(8,128)(2,1)} %wi.1, ...), custom_call_target="tpu_custom_call" | custom-call | tf_op jit(solution)/shard_map/pallas_call | solution.py:429
  64.8 1.0 %copy.16 = bf16[256,2048]{1,0:T(8,128)(2,1)} copy(bf16[256,2048]{1,0:T(8,128)(2,1)S(1)} %shard_map.136) | data formatting | bytes 2097152

commit v7 on v6

--- a/solution.py
+++ b/solution.py
@@ -26,7 +26,7 @@
     out,
     PM, OB, holder, slot, taps, route, G, ST, WIN, WKV, TB, KS, KR, OV, WV, WS, PV, PS, Q, AS, A, W,
     lsem, stsem, ixr, ixs, kvr, kvs, agr, sib, gsend, arecv, asend,
-    wloc, w1, p1, p2, wsib, wsown, wsend, osem,
+    wloc, w1, p1, p2, wsib, wsown, wsend, osem, row_sem, all_sem,
 ):
     st = lax.axis_index("st")
     tp = lax.axis_index("tp")
@@ -62,15 +62,23 @@
 
     bar = pltpu.get_barrier_semaphore()
 
-    def sig_tp(d, _):
-        pl.semaphore_signal(bar, inc=1, device_id=(st, lax.rem(tp + d, NTP)), device_id_type=MESH)
+    def signal(sem, dev):
+        pl.semaphore_signal(sem, inc=1, device_id=dev, device_id_type=MESH)
+
+    def sig_row(d, _):
+        p = lax.rem(y + d, NY) * 2 + 1
+
+        @pl.when(p != tp)
+        def _():
+            signal(bar, (st, p))
+
         return 0
 
     def sig_st(d, _):
-        pl.semaphore_signal(bar, inc=1, device_id=(lax.rem(st + d, NST), tp), device_id_type=MESH)
-        return 0
-
-    lax.fori_loop(1, NTP, sig_tp, 0)
+        signal(bar, (lax.rem(st + d, NST), y * 2))
+        return 0
+
+    lax.fori_loop(0, NY, sig_row, 0)
     lax.fori_loop(1, NST, sig_st, 0)
 
     loads = []
@@ -127,18 +135,14 @@
     pcopy = pltpu.make_async_copy(PV, PS, lsem.at[7])
     pcopy.start()
 
-    pl.semaphore_wait(bar, NTP - 1 + NST - 1)
-
-    def ix_copy(d):
-        r = lax.rem(st + d, NST)
-        return rcopy(OV.at[r], WV.at[st], ixs, ixr, (r, tp))
-
-    def ix_start(d, _):
-        ix_copy(d).start()
-        return 0
-
-    lax.fori_loop(1, NST, ix_start, 0)
-    pltpu.make_async_copy(OV.at[st], WV.at[st], ixr).start()
+    @pl.when(k == 1)
+    def _():
+        pl.semaphore_wait(bar, NTP - 1)
+        signal(row_sem, sibling)
+
+    @pl.when(k == 0)
+    def _():
+        pl.semaphore_wait(row_sem, 1)
 
     def direct(t):
         src = tokens.at[:, rows(t), :]
@@ -163,6 +167,26 @@
     direct(0)
     direct(1)
 
+    @pl.when(k == 0)
+    def _():
+        pl.semaphore_wait(bar, 2 * (NST - 1))
+        signal(all_sem, sibling)
+
+    @pl.when(k == 1)
+    def _():
+        pl.semaphore_wait(all_sem, 1)
+
+    def ix_copy(d):
+        r = lax.rem(st + d, NST)
+        return rcopy(OV.at[r], WV.at[st], ixs, ixr, (r, tp))
+
+    def ix_start(d, _):
+        ix_copy(d).start()
+        return 0
+
+    lax.fori_loop(1, NST, ix_start, 0)
+    pltpu.make_async_copy(OV.at[st], WV.at[st], ixr).start()
+
     arrived(WKV, lsem.at[1])
     arrived(ST, stsem)
 
@@ -173,14 +197,16 @@
             TB[i * 4 + j] = kv[j * PLEN : (j + 1) * PLEN]
         return 0
 
-    lax.fori_loop(0, 6, kv_body, 0)
+    lax.fori_loop(0, 3, kv_body, 0)
+    direct(2)
+    lax.fori_loop(3, 6, kv_body, 0)
 
     def send_kv():
         arrived(WV, ixr)
         c = pltpu.make_async_copy(WV, WS, lsem.at[3])
         c.start()
         c.wait()
-        lax.fori_loop(1, NST, kv_out, 0)
+        lax.fori_loop(1, 4, kv_out, 0)
         for j in range(CAP):
             KS[st, j] = TB[WS[st, 0, j]]
         pltpu.make_async_copy(KS.at[st], KR.at[pl.ds(st * CAP, CAP)], kvr).start()
@@ -323,11 +349,15 @@
             rcopy(h2, h2, gsend, agr.at[t, 2], dev_y(-1)).start()
             rcopy(g2, g2, gsend, sib.at[t], sibling).start()
 
-        @pl.when(t < 6)
+        @pl.when((t >= 1) & (t < 6))
         def _():
             direct(t + 2)
 
-        @pl.when(t == 3)
+        @pl.when(t <= 1)
+        def _():
+            lax.fori_loop(4 + 6 * t, 10 + 6 * t, kv_out, 0)
+
+        @pl.when(t == 4)
         def _():
             plane2()
 
@@ -358,16 +388,17 @@
         def _():
             project(t - 2)
 
-        @pl.when(t == 6)
+        @pl.when(t == 7)
         def _():
             arrived(KR, kvr)
             pcopy.wait()
 
-        @pl.when((t == 6) | (t == 7))
-        def _():
-            attend(range(NTP), pl.multiple_of((t - 6) * 64, 64), 64)
-            send_branch(1, (t - 6) * 64, 64)
-
+            def two(i, _):
+                attend(range(NTP), pl.multiple_of(i * 64, 64), 64)
+                send_branch(1, i * 64, 64)
+                return 0
+
+            lax.fori_loop(0, 2, two, 0)
         @pl.when(t == 8)
         def _():
             plane4()
@@ -425,6 +456,7 @@
 ):
     hbm = pl.BlockSpec(memory_space=pltpu.HBM)
     dma = pltpu.SemaphoreType.DMA
+    reg = pltpu.SemaphoreType.REGULAR
     V = pltpu.VMEM
     return pl.pallas_call(
         kernel,
@@ -457,6 +489,7 @@
             dma((8,)), dma, dma, dma, dma, dma,
             dma((8, 3)), dma((8,)), dma, dma, dma,
             dma, dma, dma, dma((4,)), dma((4,)), dma, dma, dma,
+            reg, reg,
         ],
         compiler_params=pltpu.CompilerParams(
             collective_id=0, has_side_effects=True, vmem_limit_bytes=44 * 1024 * 1024

time: 65.9 us -> 62.8 us (0.953)
  Pallas kernels: 64.8 us -> 61.7 us
    pallas_call x1, Pallas kernels: 64.8 us -> 61.7 us  [local(): pl.pallas_call(kernel, out_shape=jax.ShapeDtypeStruct((SEQ, cout.shape[1]...]
where the time goes in v7:
time: 62.8 us; the launch traced here: 62.7 us
  Pallas kernels  61.7 us (98%)
  local copies, waits for them, and re-layouts  0.97 us (2%)
    pallas_call x1, Pallas kernels, local(): pl.pallas_call(kernel, out_shape=jax.ShapeDtypeStruct((SEQ, cout.shape[1]...  61.7 us

profile of v7, /device:TPU:1, one launch (start us, length us, event | category | flops | bytes accessed | tf_op | source)
XLA Modules:
  0.0 62.7 jit_solution(15191015147587054915)
XLA Ops:
  0.0 61.7 %shard_map.136 = bf16[256,2048]{1,0:T(8,128)(2,1)S(1)} custom-call(bf16[8,256,256]{2,1,0:T(8,128)(2,1)} %bitcast.6, bf16[2048,2048]{1,0:T(8,128)(2,1)} %bitcast.5, s32[2,16]{1,0:T(2,128)} %bitcast.8, s32[2,16]{1,0:T(2,128)} %bitcast.9, bf16[2048,128]{1,0:T(8,128)(2,1)} %wq.1, bf16[2048,128]{1,0:T(8,128)(2,1)} %wo.1, bf16[2048,128]{1,0:T(8,128)(2,1)} %wi.1, ...), custom_call_target="tpu_custom_call" | custom-call | tf_op jit(solution)/shard_map/pallas_call | solution.py:461
  61.7 1.0 %copy.16 = bf16[256,2048]{1,0:T(8,128)(2,1)} copy(bf16[256,2048]{1,0:T(8,128)(2,1)S(1)} %shard_map.136) | data formatting | bytes 2097152

commit v8 on v7

--- a/solution.py
+++ b/solution.py
@@ -263,7 +263,7 @@
         arrived(SIX, p2.at[0])
         arrived(SIX, p2.at[1])
         wpass(0, 6, -1, p2.at[2], dev_b(1))
-        wpass(6, 12, 1, p2.at[2], dev_b(-1))
+        wpass(6, 12, 1, p2.at[4], dev_b(-1))
         wpass(0, 6, -1, wsib.at[1], sibling)
         wpass(6, 12, 1, wsib.at[1], sibling)
 
@@ -273,8 +273,10 @@
         wpass(0, 6, 1, wsib.at[2], sibling)
 
     def plane5():
-        arrived(TWELVE, p2.at[2])
-        wpass(0, 12, 2, wsib.at[3], sibling)
+        arrived(SIX, p2.at[2])
+        wpass(0, 6, 2, wsib.at[3], sibling)
+        arrived(SIX, p2.at[4])
+        wpass(6, 12, 2, wsib.at[3], sibling)
 
     plane1()
     lax.fori_loop(6, 8, kv_body, 0)
@@ -361,14 +363,10 @@
         def _():
             plane2()
 
-        @pl.when(t == 5)
+        @pl.when(t == 6)
         def _():
             wpass(6, 12, 0, p2.at[3], dev_b(1))
             wpass(0, 6, 0, p2.at[3], dev_b(-1))
-
-        @pl.when(t == 7)
-        def _():
-            plane3()
 
         def opposite(u):
             g = G.at[gblk(2), :, rows(u), :]
@@ -390,6 +388,7 @@
 
         @pl.when(t == 7)
         def _():
+            plane3()
             arrived(KR, kvr)
             pcopy.wait()
 
@@ -488,7 +487,7 @@
             V((NST, 2, 4, 2, 128, 128), BF16),
             dma((8,)), dma, dma, dma, dma, dma,
             dma((8, 3)), dma((8,)), dma, dma, dma,
-            dma, dma, dma, dma((4,)), dma((4,)), dma, dma, dma,
+            dma, dma, dma, dma((5,)), dma((4,)), dma, dma, dma,
             reg, reg,
         ],
         compiler_params=pltpu.CompilerParams(

time: 62.8 us -> 62.5 us (level)
  no operation moved by 1% of the time
where the time goes in v8:
time: 62.5 us; the launch traced here: 62.4 us
  Pallas kernels  61.4 us (98%)
  local copies, waits for them, and re-layouts  0.97 us (2%)
    pallas_call x1, Pallas kernels, local(): pl.pallas_call(kernel, out_shape=jax.ShapeDtypeStruct((SEQ, cout.shape[1]...  61.4 us

profile of v8, /device:TPU:1, one launch (start us, length us, event | category | flops | bytes accessed | tf_op | source)
XLA Modules:
  0.0 62.4 jit_solution(14371200440835440749)
XLA Ops:
  0.0 61.4 %shard_map.136 = bf16[256,2048]{1,0:T(8,128)(2,1)S(1)} custom-call(bf16[8,256,256]{2,1,0:T(8,128)(2,1)} %bitcast.6, bf16[2048,2048]{1,0:T(8,128)(2,1)} %bitcast.5, s32[2,16]{1,0:T(2,128)} %bitcast.8, s32[2,16]{1,0:T(2,128)} %bitcast.9, bf16[2048,128]{1,0:T(8,128)(2,1)} %wq.1, bf16[2048,128]{1,0:T(8,128)(2,1)} %wo.1, bf16[2048,128]{1,0:T(8,128)(2,1)} %wi.1, ...), custom_call_target="tpu_custom_call" | custom-call | tf_op jit(solution)/shard_map/pallas_call | solution.py:460
  61.4 1.0 %copy.16 = bf16[256,2048]{1,0:T(8,128)(2,1)} copy(bf16[256,2048]{1,0:T(8,128)(2,1)S(1)} %shard_map.136) | data formatting | bytes 2097152

commit v9 on v8

--- a/solution.py
+++ b/solution.py
@@ -261,8 +261,8 @@
 
     def plane3():
         arrived(SIX, p2.at[0])
+        wpass(0, 6, -1, p2.at[2], dev_b(1))
         arrived(SIX, p2.at[1])
-        wpass(0, 6, -1, p2.at[2], dev_b(1))
         wpass(6, 12, 1, p2.at[4], dev_b(-1))
         wpass(0, 6, -1, wsib.at[1], sibling)
         wpass(6, 12, 1, wsib.at[1], sibling)

time: 62.5 us -> 62.5 us (level)
  no operation moved by 1% of the time
where the time goes in v9:
time: 62.5 us; the launch traced here: 62.4 us
  Pallas kernels  61.4 us (98%)
  local copies, waits for them, and re-layouts  0.97 us (2%)
    pallas_call x1, Pallas kernels, local(): pl.pallas_call(kernel, out_shape=jax.ShapeDtypeStruct((SEQ, cout.shape[1]...  61.4 us

profile of v9, /device:TPU:1, one launch (start us, length us, event | category | flops | bytes accessed | tf_op | source)
XLA Modules:
  0.0 62.4 jit_solution(1200527289423187603)
XLA Ops:
  0.0 61.4 %shard_map.136 = bf16[256,2048]{1,0:T(8,128)(2,1)S(1)} custom-call(bf16[8,256,256]{2,1,0:T(8,128)(2,1)} %bitcast.6, bf16[2048,2048]{1,0:T(8,128)(2,1)} %bitcast.5, s32[2,16]{1,0:T(2,128)} %bitcast.8, s32[2,16]{1,0:T(2,128)} %bitcast.9, bf16[2048,128]{1,0:T(8,128)(2,1)} %wq.1, bf16[2048,128]{1,0:T(8,128)(2,1)} %wo.1, bf16[2048,128]{1,0:T(8,128)(2,1)} %wi.1, ...), custom_call_target="tpu_custom_call" | custom-call | tf_op jit(solution)/shard_map/pallas_call | solution.py:460
  61.4 1.0 %copy.16 = bf16[256,2048]{1,0:T(8,128)(2,1)} copy(bf16[256,2048]{1,0:T(8,128)(2,1)S(1)} %shard_map.136) | data formatting | bytes 2097152

commit v10 on v8

--- a/solution.py
+++ b/solution.py
@@ -15,7 +15,7 @@
 NST = 16
 NTP = 8
 STEP = 32
-WIDE = 1024
+WIDE = 2048
 MESH = pl.DeviceIdType.MESH
 F32 = jnp.float32
 BF16 = jnp.bfloat16

time: 62.5 us -> 62.5 us (level)
  no operation moved by 1% of the time
where the time goes in v10:
time: 62.5 us; the launch traced here: 62.4 us
  Pallas kernels  61.4 us (98%)
  local copies, waits for them, and re-layouts  0.97 us (2%)
    pallas_call x1, Pallas kernels, local(): pl.pallas_call(kernel, out_shape=jax.ShapeDtypeStruct((SEQ, cout.shape[1]...  61.4 us

profile of v10, /device:TPU:1, one launch (start us, length us, event | category | flops | bytes accessed | tf_op | source)
XLA Modules:
  0.0 62.4 jit_solution(12333272234050104593)
XLA Ops:
  0.0 61.4 %shard_map.136 = bf16[256,2048]{1,0:T(8,128)(2,1)S(1)} custom-call(bf16[8,256,256]{2,1,0:T(8,128)(2,1)} %bitcast.6, bf16[2048,2048]{1,0:T(8,128)(2,1)} %bitcast.5, s32[2,16]{1,0:T(2,128)} %bitcast.8, s32[2,16]{1,0:T(2,128)} %bitcast.9, bf16[2048,128]{1,0:T(8,128)(2,1)} %wq.1, bf16[2048,128]{1,0:T(8,128)(2,1)} %wo.1, bf16[2048,128]{1,0:T(8,128)(2,1)} %wi.1, ...), custom_call_target="tpu_custom_call" | custom-call | tf_op jit(solution)/shard_map/pallas_call | solution.py:460
  61.4 1.0 %copy.16 = bf16[256,2048]{1,0:T(8,128)(2,1)} copy(bf16[256,2048]{1,0:T(8,128)(2,1)S(1)} %shard_map.136) | data formatting | bytes 2097152
